TPU v7x, 32 devices: a whole 2x2x4 slice. The times are simulated.
32 devices in a mesh: rep: 4 (over z), fs: 4 (over y, x), tp: 2 (over core).
Axes of the slice: x: 2, y: 2, z: 4, core: 2. Of those that a mesh axis runs over, the one named last changes fastest.
Arguments:
- residual: bfloat16 [16, 256, 2048], P(('rep', 'fs'), None, 'tp'), may hold values from -6 to 6
- queries: bfloat16 [16, 256, 2048], P(('rep', 'fs'), None, 'tp'), may hold values from -6 to 6
- key_matrix: bfloat16 [16, 256, 2048], P(('rep', 'fs'), None, 'tp'), may hold values from -6 to 6
- value_matrix: bfloat16 [16, 256, 2048], P(('rep', 'fs'), None, 'tp'), may hold values from -6 to 6
- decay_logodds: float32 [16, 256, 2048], P(('rep', 'fs'), None, 'tp'), may hold values from -3.4 to 8.9, as said below
- decay_surge: float32 [16, 256, 8], P(('rep', 'fs'), None, 'tp'), may hold values from -2.1 to 0, as said below
- head_norm_gain: float32 [256], replicated, may hold values from 0.1 to 1.9
- output_matrix: float32 [2048, 2048], P('fs', 'tp'), may hold values from -0.125 to 0.125
- output_column_scale: float32 [2048], P('tp'), may hold values from 0.5 to 2
- premix_norm_gain: float32 [2048], replicated, may hold values from 0.1 to 1.9
- gate_matrix: float32 [2048, 2816], P('fs', 'tp'), may hold values from -0.125 to 0.125
- gate_column_scale: float32 [2816], P('tp'), may hold values from 0.5 to 2
- up_matrix: float32 [2048, 2816], P('fs', 'tp'), may hold values from -0.125 to 0.125
- up_column_scale: float32 [2816], P('tp'), may hold values from 0.5 to 2
- down_matrix: float32 [2048, 2816], P('fs', 'tp'), may hold values from -0.109375 to 0.109375
- down_column_scale: float32 [2048], P('tp'), may hold values from 0.5 to 2
Outputs:
- layer_out: bfloat16 [16, 256, 2048], P(('rep', 'fs'), None, 'tp')
Inputs may be any that keep to these rules, and one draw needn't show every extreme that they name: `decay_logodds`: log-odds of a key channel's decay. `decay_surge`: non-positive log-factors of a head's state.
All inputs are finite; a program needn't handle non-finite values.
Results may differ from a plain program's by a relative error of at most 0.018.
Values may be sent and summed in bfloat16 or wider, within the bound.
A program may use at most 128 MiB of HBM per device.

v0:
```python
import functools

import jax
import jax.numpy as jnp
from jax import lax
from jax.experimental import pallas as pl
from jax.experimental.pallas import tpu as pltpu
from jax.sharding import PartitionSpec as P

BLOCK = 64


epsilon = 1e-06
softness_factor = 16.0
highest = lax.Precision.HIGHEST


def attend_head(q, k, v, logodds, surge, gain):
    tokens, width = q.shape
    blocks = tokens // BLOCK
    mid = BLOCK // 2 - 1
    decay = (
        jnp.minimum(logodds, 0.0) - jnp.log1p(jnp.exp(-jnp.abs(logodds)))
    ) * (1.0 / softness_factor) + surge
    row = lax.broadcasted_iota(jnp.int32, (BLOCK, BLOCK), 0)
    col = lax.broadcasted_iota(jnp.int32, (BLOCK, BLOCK), 1)
    tri = jnp.where(row >= col, 1.0, 0.0).astype(jnp.bfloat16)
    q = q.astype(jnp.float32) * width ** (-0.5)
    k = k.astype(jnp.float32)
    high = decay.astype(jnp.bfloat16)
    low = (decay - high.astype(jnp.float32)).astype(jnp.bfloat16)
    pieces = []
    for n in range(blocks):
        rows = slice(n * BLOCK, (n + 1) * BLOCK)
        running = jnp.dot(tri, high[rows], preferred_element_type=jnp.float32) + jnp.dot(
            tri, low[rows], preferred_element_type=jnp.float32
        )
        before = running - decay[rows]
        center = running[mid : mid + 1]
        end = running[BLOCK - 1 : BLOCK]
        to_center = jnp.exp(center)
        from_center = jnp.exp(end - center)
        q_forward = q[rows] * jnp.exp(running - center)
        k_forward = k[rows] * jnp.exp(center - running)
        q_backward = q[rows] * jnp.exp(center - before)
        k_backward = k[rows] * jnp.exp(before - center)
        half = jnp.bfloat16
        scores = jnp.where(
            row >= col, by_rows(q_forward.astype(half), k_forward.astype(half)), 0.0
        ) + jnp.where(row <= col, by_rows(q_backward.astype(half), k_backward.astype(half)), 0.0)
        inner = jnp.dot(scores.astype(half), v[rows], preferred_element_type=jnp.float32)
        pieces.append(
            (
                inner,
                (q_forward * to_center).astype(half),
                (q_backward * from_center).astype(half),
                by_columns(v[rows], (k_forward * from_center).astype(half)),
                by_columns(v[rows], (k_backward * to_center).astype(half)),
                jnp.exp(end),
            )
        )
    totals = [piece[0] for piece in pieces]
    state = None
    for n in range(blocks):
        if state is not None:
            totals[n] = totals[n] + by_rows(pieces[n][1], state.astype(jnp.bfloat16))
        state = pieces[n][3] if state is None else pieces[n][5] * state + pieces[n][3]
    state = None
    for n in reversed(range(blocks)):
        if state is not None:
            totals[n] = totals[n] + by_rows(pieces[n][2], state.astype(jnp.bfloat16))
        state = pieces[n][4] if state is None else pieces[n][5] * state + pieces[n][4]
    attended = jnp.concatenate(totals, axis=0)
    scale = lax.rsqrt(jnp.mean(attended * attended, axis=-1, keepdims=True) + epsilon)
    return (attended * scale * gain).astype(jnp.bfloat16)


def by_columns(left, right):
    return lax.dot_general(
        left, right, (((0,), (0,)), ((), ())), preferred_element_type=jnp.float32
    )


def attend_kernel(head_total, q_ref, k_ref, v_ref, lo_ref, sg_ref, gain_ref, out_ref):
    width = q_ref.shape[1] // head_total
    value_width = v_ref.shape[1] // head_total
    for h in range(head_total):
        keys = slice(h * width, (h + 1) * width)
        values = slice(h * value_width, (h + 1) * value_width)
        out_ref[:, values] = attend_head(
            q_ref[:, keys],
            k_ref[:, keys],
            v_ref[:, values],
            lo_ref[:, keys],
            sg_ref[:, h : h + 1],
            gain_ref[...],
        )


def linear_attend(queries, key_matrix, value_matrix, decay_logodds, decay_surge, head_norm_gain):
    _, token_length, head_total = decay_surge.shape
    outs = [
        pl.pallas_call(
            functools.partial(attend_kernel, head_total),
            out_shape=jax.ShapeDtypeStruct(value_matrix.shape[1:], jnp.bfloat16),
            in_specs=[pl.BlockSpec(memory_space=pltpu.VMEM)] * 6,
            out_specs=pl.BlockSpec(memory_space=pltpu.VMEM),
            cost_estimate=pl.CostEstimate(
                flops=10**9, bytes_accessed=4 * 10**6, transcendentals=10**6
            ),
        )(
            queries[b], key_matrix[b], value_matrix[b], decay_logodds[b], decay_surge[b],
            head_norm_gain.reshape(1, -1),
        )
        for b in range(queries.shape[0])
    ]
    return jnp.concatenate(outs, axis=0)


def by_rows(left, right):
    return lax.dot_general(
        left, right, (((1,), (1,)), ((), ())), preferred_element_type=jnp.float32
    )


def body(
    residual,
    queries,
    key_matrix,
    value_matrix,
    decay_logodds,
    decay_surge,
    head_norm_gain,
    output_matrix,
    output_column_scale,
    premix_norm_gain,
    gate_matrix,
    gate_column_scale,
    up_matrix,
    up_column_scale,
    down_matrix,
    down_column_scale,
):
    sequence_batch, token_length, local_width = residual.shape
    row_count = sequence_batch * token_length
    normalized_rows = linear_attend(
        queries, key_matrix, value_matrix, decay_logodds, decay_surge, head_norm_gain
    )
    out_half = output_matrix.astype(jnp.bfloat16)
    out_full = lax.all_gather(out_half, "fs", axis=0, tiled=True)
    mix_terms = by_rows(normalized_rows, out_full)
    mix_total = lax.psum_scatter(
        mix_terms.astype(jnp.bfloat16), "tp", scatter_dimension=1, tiled=True
    ).astype(jnp.float32)
    own_rows = residual.reshape(row_count, local_width).astype(jnp.float32)
    updated = (own_rows + output_column_scale * mix_total).astype(jnp.bfloat16)
    features = lax.all_gather(updated, "tp", axis=1, tiled=True)
    wide_rows = features.astype(jnp.float32)
    factor = lax.rsqrt(jnp.mean(wide_rows * wide_rows, axis=-1, keepdims=True) + epsilon)
    normin = (wide_rows * factor * premix_norm_gain).astype(jnp.bfloat16)
    gate_half = gate_matrix.astype(jnp.bfloat16)
    up_half = up_matrix.astype(jnp.bfloat16)
    down_half = down_matrix.astype(jnp.bfloat16)
    gate_full, up_full, down_full = (
        lax.all_gather(gate_half, "fs", axis=0, tiled=True),
        lax.all_gather(up_half, "fs", axis=0, tiled=True),
        lax.all_gather(down_half, "fs", axis=0, tiled=True),
    )
    gate_pre = jnp.dot(normin, gate_full, preferred_element_type=jnp.float32)
    up_pre = jnp.dot(normin, up_full, preferred_element_type=jnp.float32)
    hidden = (jax.nn.silu(gate_pre * gate_column_scale) * (up_pre * up_column_scale)).astype(
        jnp.bfloat16
    )
    down_terms = by_rows(hidden, down_full)
    down_total = lax.psum_scatter(
        down_terms.astype(jnp.bfloat16), "tp", scatter_dimension=1, tiled=True
    ).astype(jnp.float32)
    result = (updated.astype(jnp.float32) + down_column_scale * down_total).astype(jnp.bfloat16)
    return result.reshape(sequence_batch, token_length, local_width)


def exchange_kernel(axis, n, spread, count, *refs):
    ins, outs = refs[:count], refs[count : 2 * count]
    send_sem, recv_sem = refs[2 * count :]
    me = lax.axis_index(axis)
    barrier = pltpu.get_barrier_semaphore()
    for step in range(1, n):
        pl.semaphore_signal(
            barrier,
            inc=1,
            device_id={axis: lax.rem(me + step, n)},
            device_id_type=pl.DeviceIdType.MESH,
        )
    pl.semaphore_wait(barrier, n - 1)
    copies = []
    for step in range(1, n):
        peer = lax.rem(me + step, n)
        for c in range(count):
            copy = pltpu.make_async_remote_copy(
                src_ref=ins[c].at[peer] if spread else ins[c],
                dst_ref=outs[c].at[me],
                send_sem=send_sem.at[c, step - 1],
                recv_sem=recv_sem.at[c, step - 1],
                device_id={axis: peer},
                device_id_type=pl.DeviceIdType.MESH,
            )
            copy.start()
            copies.append(copy)
    for c in range(count):
        outs[c][me] = ins[c][me] if spread else ins[c][...]
    for copy in copies:
        copy.wait()


def exchange(arrays, axis, n, spread, call):
    count = len(arrays)
    shapes = [a.shape if spread else (n,) + a.shape for a in arrays]
    return pl.pallas_call(
        functools.partial(exchange_kernel, axis, n, spread, count),
        out_shape=[jax.ShapeDtypeStruct(d, a.dtype) for d, a in zip(shapes, arrays)],
        in_specs=[pl.BlockSpec(memory_space=pltpu.VMEM)] * count,
        out_specs=[pl.BlockSpec(memory_space=pltpu.VMEM)] * count,
        scratch_shapes=[
            pltpu.SemaphoreType.DMA((count, n - 1)),
            pltpu.SemaphoreType.DMA((count, n - 1)),
        ],
        compiler_params=pltpu.CompilerParams(collective_id=call, has_side_effects=True),
        cost_estimate=pl.CostEstimate(
            flops=10**9, bytes_accessed=2 * 10**7, transcendentals=0
        ),
    )(*arrays)


def send(source, target, sems, index, device):
    copy = pltpu.make_async_remote_copy(
        src_ref=source,
        dst_ref=target,
        send_sem=sems[0].at[index],
        recv_sem=sems[1].at[index],
        device_id=device,
        device_id_type=pl.DeviceIdType.MESH,
    )
    copy.start()
    return copy


def greet(devices):
    barrier = pltpu.get_barrier_semaphore()
    for device in devices:
        pl.semaphore_signal(
            barrier, inc=1, device_id=device, device_id_type=pl.DeviceIdType.MESH
        )
    pl.semaphore_wait(barrier, len(devices))


def gather_kernel(share, x_ref, out_ref, *sems):
    me, tp = lax.axis_index("fs"), lax.axis_index("tp")
    near = me + 1 - 2 * lax.rem(me, 2)
    far = lax.rem(me + 2, 4)
    corner = lax.rem(near + 2, 4)
    to_near, to_far, to_pair = {"fs": near}, {"fs": far}, {"tp": 1 - tp}
    greet([to_near, to_far] + ([to_pair] if share else []))
    own = out_ref.at[tp] if share else out_ref
    rows = x_ref.shape[0] // 2
    upper, lower = pl.ds(0, rows), pl.ds(rows, rows)
    near_upper = send(x_ref.at[upper], own.at[me, upper], sems, 0, to_near)
    far_lower = send(x_ref.at[lower], own.at[me, lower], sems, 1, to_far)
    near_lower = send(x_ref.at[lower], own.at[me, lower], sems, 2, to_near)
    far_upper = send(x_ref.at[upper], own.at[me, upper], sems, 3, to_far)
    copies = [near_upper, far_lower, near_lower, far_upper]
    shared = [send(x_ref, own.at[me], sems, 6, to_pair)] if share else []
    own[me] = x_ref[...]
    near_upper.wait_recv()
    corner_upper = send(own.at[near, upper], own.at[near, upper], sems, 4, to_far)
    far_lower.wait_recv()
    corner_lower = send(own.at[far, lower], own.at[far, lower], sems, 5, to_near)
    near_lower.wait_recv()
    if share:
        shared.append(send(own.at[near], own.at[near], sems, 7, to_pair))
    far_upper.wait_recv()
    if share:
        shared.append(send(own.at[far], own.at[far], sems, 8, to_pair))
    corner_upper.wait_recv()
    corner_lower.wait_recv()
    if share:
        shared.append(send(own.at[corner], own.at[corner], sems, 9, to_pair))
    for copy in copies + [corner_upper, corner_lower]:
        copy.wait_send()
    for copy in shared:
        copy.wait()


def gather(x, n_fs, n_tp, share, call):
    shape = ((n_tp,) if share else ()) + (n_fs,) + x.shape
    return pl.pallas_call(
        functools.partial(gather_kernel, share),
        out_shape=jax.ShapeDtypeStruct(shape, x.dtype),
        in_specs=[pl.BlockSpec(memory_space=pltpu.VMEM)],
        out_specs=pl.BlockSpec(memory_space=pltpu.VMEM),
        scratch_shapes=[pltpu.SemaphoreType.DMA((10,)), pltpu.SemaphoreType.DMA((10,))],
        compiler_params=pltpu.CompilerParams(collective_id=call, has_side_effects=True),
        cost_estimate=pl.CostEstimate(
            flops=10**9, bytes_accessed=2 * 10**7, transcendentals=0
        ),
    )(x)


def reduce_kernel(n, terms_ref, back_ref, part_ref, total_ref, *sems):
    me, tp = lax.axis_index("fs"), lax.axis_index("tp")
    steps = list(range(1, n)) + [0]
    peers = [lax.rem(me + step, n) for step in range(n)]
    greet([{"fs": peers[step]} for step in range(1, n)] + [{"tp": 1 - tp}])
    pairs = {
        step: send(
            terms_ref.at[1 - tp, peers[step]], part_ref.at[peers[step]], sems, step, {"tp": 1 - tp}
        )
        for step in steps
    }
    copies = []
    for step in steps:
        peer = peers[step]
        pairs[step].wait_recv()
        total = terms_ref[tp, peer].astype(jnp.float32) + part_ref[peer].astype(jnp.float32)
        if step == 0:
            back_ref[me] = total.astype(back_ref.dtype)
        else:
            total_ref[peer] = total.astype(back_ref.dtype)
            copies.append(
                send(total_ref.at[peer], back_ref.at[me], sems, n + step, {"fs": peer})
            )
    for step in steps:
        pairs[step].wait_send()
    for copy in copies:
        copy.wait()


def reduce_back(terms, n_fs, call):
    shape = terms.shape[1:]
    return pl.pallas_call(
        functools.partial(reduce_kernel, n_fs),
        out_shape=jax.ShapeDtypeStruct(shape, terms.dtype),
        in_specs=[pl.BlockSpec(memory_space=pltpu.VMEM)],
        out_specs=pl.BlockSpec(memory_space=pltpu.VMEM),
        scratch_shapes=[
            pltpu.VMEM(shape, terms.dtype),
            pltpu.VMEM(shape, terms.dtype),
            pltpu.SemaphoreType.DMA((2 * n_fs,)),
            pltpu.SemaphoreType.DMA((2 * n_fs,)),
        ],
        compiler_params=pltpu.CompilerParams(collective_id=call, has_side_effects=True),
        cost_estimate=pl.CostEstimate(
            flops=10**9, bytes_accessed=2 * 10**7, transcendentals=0
        ),
    )(terms)


def pack_kernel(n, units, padded, *refs):
    matrices, out_ref, held, sems = refs[:3], refs[3], refs[4], refs[5]
    slab = held.shape[1]
    rows = pl.ds(pl.multiple_of(lax.axis_index("rep") * slab, slab), slab)
    copies = [
        pltpu.make_async_copy(matrix.at[rows], held.at[m], sems.at[m])
        for m, matrix in enumerate(matrices)
    ]
    for copy in copies:
        copy.start()
    for m, copy in enumerate(copies):
        copy.wait()
        for j in range(n):
            own = held[m, :, j * units : (j + 1) * units]
            if padded > units:
                fill = jnp.zeros((slab, padded - units), own.dtype)
                own = jnp.concatenate([own, fill], axis=1)
            out_ref[j, :, m * padded : (m + 1) * padded] = own.astype(out_ref.dtype)


def pack(matrices, n, units, padded, slab):
    return pl.pallas_call(
        functools.partial(pack_kernel, n, units, padded),
        out_shape=jax.ShapeDtypeStruct((n, slab, 3 * padded), jnp.bfloat16),
        in_specs=[pl.BlockSpec(memory_space=pl.ANY)] * 3,
        out_specs=pl.BlockSpec(memory_space=pltpu.VMEM),
        scratch_shapes=[
            pltpu.VMEM((3, slab, matrices[0].shape[1]), jnp.float32),
            pltpu.SemaphoreType.DMA((3,)),
        ],
        cost_estimate=pl.CostEstimate(
            flops=10**6, bytes_accessed=4 * 10**6, transcendentals=0
        ),
    )(*matrices)


def moving_body(
    sizes,
    residual,
    queries,
    key_matrix,
    value_matrix,
    decay_logodds,
    decay_surge,
    head_norm_gain,
    output_matrix,
    output_column_scale,
    premix_norm_gain,
    gate_matrix,
    gate_column_scale,
    up_matrix,
    up_column_scale,
    down_matrix,
    down_column_scale,
):
    n_rep, n_fs, n_tp = sizes
    half = jnp.bfloat16
    sequence_batch, token_length, local_width = residual.shape
    row_count = sequence_batch * token_length
    width = local_width * n_tp
    own_width = output_matrix.shape[0]
    part = own_width // n_tp
    units = gate_matrix.shape[1] // n_fs
    padded = -(-units // 128) * 128
    slab = own_width // n_rep
    rep, fs, tp = lax.axis_index("rep"), lax.axis_index("fs"), lax.axis_index("tp")

    weights = pack((gate_matrix, up_matrix, down_matrix), n_fs, units, padded, slab)
    own_rows = residual.reshape(row_count, local_width)
    both_rows, both_scale = exchange(
        [own_rows, output_column_scale.reshape(1, local_width)], "tp", n_tp, False, 1
    )
    wide = jnp.transpose(both_rows, (1, 0, 2)).reshape(row_count, n_fs, n_tp, part)
    mine = lax.dynamic_index_in_dim(wide, tp, axis=2, keepdims=False)
    got_weights, got_rows = exchange(
        [weights, jnp.transpose(mine, (1, 0, 2))], "fs", n_fs, True, 2
    )
    all_weights = lax.all_gather(got_weights, "rep", axis=0, tiled=False)
    all_weights = jnp.transpose(all_weights, (1, 0, 2, 3)).reshape(width, 3 * padded)

    normalized_rows = linear_attend(
        queries, key_matrix, value_matrix, decay_logodds, decay_surge, head_norm_gain
    )
    gathered = gather(normalized_rows, n_fs, n_tp, False, 3)
    group_rows = n_fs * row_count
    mix_terms = by_rows(gathered.reshape(group_rows, -1), output_matrix.astype(half)).astype(half)
    mix_split = jnp.transpose(mix_terms.reshape(group_rows, n_tp, part), (1, 0, 2))
    (mix_parts,) = exchange([mix_split], "tp", n_tp, True, 4)
    mixed = jnp.sum(mix_parts.astype(jnp.float32), axis=0)
    out_scale = lax.dynamic_index_in_dim(
        lax.dynamic_index_in_dim(both_scale.reshape(n_fs, n_tp, part), fs, 0, False), tp, 0, False
    )
    piece = got_rows.reshape(group_rows, part).astype(jnp.float32) + out_scale * mixed
    everywhere = gather(piece.astype(half), n_fs, n_tp, True, 5)
    updated = jnp.transpose(everywhere, (2, 1, 0, 3)).reshape(group_rows, width)
    wide_rows = updated.astype(jnp.float32)
    factor = lax.rsqrt(jnp.mean(wide_rows * wide_rows, axis=-1, keepdims=True) + epsilon)
    normin = (wide_rows * factor * premix_norm_gain).astype(half)

    def unit_scale(scale):
        own = lax.dynamic_index_in_dim(scale.reshape(n_fs, units), fs, 0, False)
        return jnp.pad(own, (0, padded - units))

    both = jnp.dot(normin, all_weights[:, : 2 * padded], preferred_element_type=jnp.float32)
    gate_pre = both[:, :padded] * unit_scale(gate_column_scale)
    up_pre = both[:, padded:] * unit_scale(up_column_scale)
    hidden = (jax.nn.silu(gate_pre) * up_pre).astype(half)
    down_terms = jnp.concatenate(
        [
            by_rows(
                hidden, all_weights[t * local_width : (t + 1) * local_width, 2 * padded :]
            ).astype(half)[None]
            for t in range(n_tp)
        ],
        axis=0,
    )
    down_back = reduce_back(
        down_terms.reshape(n_tp, n_fs, row_count, local_width), n_fs, 7
    )
    down_total = jnp.sum(down_back.astype(jnp.float32), axis=0)
    own_updated = lax.dynamic_slice(
        updated, (fs * row_count, tp * local_width), (row_count, local_width)
    )
    result = (own_updated.astype(jnp.float32) + down_column_scale * down_total).astype(half)
    return result.reshape(sequence_batch, token_length, local_width)


def chosen_body(mesh):
    sizes = tuple(mesh.shape[name] for name in ("rep", "fs", "tp"))
    n_rep, n_fs, n_tp = sizes

    def run(*args):
        residual, output_matrix, gate_matrix = args[0], args[7], args[10]
        weights = output_matrix.size + 3 * gate_matrix.size
        rows = residual.shape[0] * residual.shape[1]
        moved = 3 * rows * residual.shape[2] + 3 * gate_matrix.size // n_rep
        fits = (
            n_fs == 4
            and n_tp == 2
            and output_matrix.shape[0] % (128 * n_tp) == 0
            and output_matrix.shape[0] % (16 * n_rep) == 0
        )
        if fits and moved < weights:
            return moving_body(sizes, *args)
        return body(*args)

    return run


def solution(mesh):
    return jax.shard_map(
        chosen_body(mesh),
        mesh=mesh,
        in_specs=(
            P(("rep", "fs"), None, "tp"),
            P(("rep", "fs"), None, "tp"),
            P(("rep", "fs"), None, "tp"),
            P(("rep", "fs"), None, "tp"),
            P(("rep", "fs"), None, "tp"),
            P(("rep", "fs"), None, "tp"),
            P(),
            P("fs", "tp"),
            P("tp"),
            P(),
            P("fs", "tp"),
            P("tp"),
            P("fs", "tp"),
            P("tp"),
            P("fs", "tp"),
            P("tp"),
        ),
        out_specs=P(("rep", "fs"), None, "tp"),
        check_vma=False,
    )
```

profile of v0, /device:TPU:1, one launch (start us, length us, event | category | flops | bytes accessed | tf_op | source)
XLA Modules:
  0.0 187.1 jit_solution(3790522598793054070)
XLA Ops:
  6.5 4.0 %shard_map.155 = (bf16[2,256,1024]{2,1,0:T(8,128)(2,1)}, f32[2,1,1024]{2,1,0:T(1,128)}) custom-call(bf16[256,1024]{1,0:T(8,128)(2,1)} %bitcast.51, f32[1,1024]{1,0:T(1,128)} %bitcast.55), custom_call_target="tpu_custom_call" | custom-call | flops 1000000000 | bytes 20000000 | tf_op jit(solution)/shard_map/pallas_call | solution.py:218
  10.5 1.5 copy.31
  12.1 1.0 copy.32
  13.1 2.7 %shard_map.154.refs_0_ = bf16[4,128,1152]{2,1,0:T(8,128)(2,1)} custom-call(f32[512,1408]{1,0:T(8,128)} %refs_0_.1, f32[512,1408]{1,0:T(8,128)} %refs_1_.1, f32[512,1408]{1,0:T(8,128)} %refs_2_.1), custom_call_target="tpu_custom_call" | custom-call | flops 1000000 | bytes 4000000 | tf_op jit(solution)/shard_map/pallas_call | solution.py:378
  15.9 25.7 %shard_map.156 = (bf16[4,128,1152]{2,1,0:T(8,128)(2,1)}, bf16[4,256,256]{2,1,0:T(8,128)(2,1)}) custom-call(bf16[4,128,1152]{2,1,0:T(8,128)(2,1)} %shard_map.154.refs_0_, bf16[4,256,256]{2,1,0:T(8,128)(2,1)} %bitcast.47), custom_call_target="tpu_custom_call" | custom-call | flops 1000000000 | bytes 20000000 | tf_op jit(solution)/shard_map/pallas_call | solution.py:218
  41.6 0.0 all-gather.3.cloned.1.call-update
  41.6 0.1 reshape.67
  41.7 0.1 reshape.68
  41.9 0.8 copy.33
  42.7 8.2 %shard_map.157.x_ref = bf16[256,1024]{1,0:T(8,128)(2,1)} custom-call(bf16[256,1024]{1,0:T(8,128)(2,1)} %bitcast.52, bf16[256,1024]{1,0:T(8,128)(2,1)} %bitcast.53, bf16[256,1024]{1,0:T(8,128)(2,1)} %bitcast.54, f32[256,1024]{1,0:T(8,128)} %bitcast.50, f32[256,4]{1,0:T(8,128)} %bitcast.48, f32[1,256]{1,0:T(1,128)} %bitcast.56), custom_call_target="tpu_custom_call" | custom-call | flops 1000000000 | bytes 4000000 | tf_op jit(solution)/shard_map/pallas_call | solution.py:103
  51.0 20.8 %shard_map.158 = bf16[4,256,1024]{2,1,0:T(8,128)(2,1)} custom-call(bf16[256,1024]{1,0:T(8,128)(2,1)} %shard_map.157.x_ref), custom_call_target="tpu_custom_call" | custom-call | flops 1000000000 | bytes 20000000 | tf_op jit(solution)/shard_map/pallas_call | solution.py:295
  71.8 2.9 %convolution_convert_fusion.2 = bf16[1024,512]{0,1:T(8,128)(2,1)S(1)} fusion(bf16[1024,1024]{1,0:T(8,128)(2,1)} %bitcast.57, f32[512,1024]{1,0:T(8,128)S(1)} %copy-done.7), kind=kOutput, calls=%fused_computation.15 | convolution fusion | flops 1074790400 | bytes 5242880 | tf_op jit(solution)/shard_map/dot_general | solution.py:121
  74.6 1.3 copy.34
  76.0 5.8 %shard_map.159 = bf16[2,1024,256]{2,1,0:T(8,128)(2,1)} custom-call(bf16[2,1024,256]{2,1,0:T(8,128)(2,1)} %bitcast.46), custom_call_target="tpu_custom_call" | custom-call | flops 1000000000 | bytes 20000000 | tf_op jit(solution)/shard_map/pallas_call | solution.py:218
  81.8 1.5 convert_reduce_fusion.1
  83.4 1.0 fusion.6.x_ref
  84.3 24.6 %shard_map.160 = bf16[2,4,1024,256]{3,2,1,0:T(8,128)(2,1)} custom-call(bf16[1024,256]{1,0:T(8,128)(2,1)} %fusion.6.x_ref), custom_call_target="tpu_custom_call" | custom-call | flops 1000000000 | bytes 20000000 | tf_op jit(solution)/shard_map/pallas_call | solution.py:295
  108.9 6.3 %copy.35 = bf16[1024,4,2,256]{0,3,2,1:T(8,128)(2,1)} copy(bf16[1024,4,2,256]{3,0,1,2:T(8,128)(2,1)} %bitcast.34) | data formatting | bytes 8388608 | tf_op jit(solution)/shard_map/transpose | solution.py:451
  115.2 1.1 dynamic_slice.22
  116.3 0.2 copy.38
  116.5 3.1 %multiply_reduce_fusion = f32[1024]{0:T(1024)S(1)} fusion(bf16[2,4,1024,256]{3,2,1,0:T(8,128)(2,1)} %shard_map.160), kind=kLoop, calls=%fused_computation.1 | loop fusion | flops 6290432 | bytes 4198400 | tf_op jit(solution)/shard_map/reduce_sum | solution.py:453
  119.6 12.5 %all-gather.3.cloned.1.call-done = bf16[16,128,1152]{2,1,0:T(8,128)(2,1)} async-done(((bf16[4,128,1152]{2,1,0:T(8,128)(2,1)}), bf16[16,128,1152]{2,1,0:T(8,128)(2,1)}) %all-gather.3.cloned.1.call-update) | async-done | bytes 4718608 | tf_op jit(solution)/shard_map/all_gather | solution.py:434
  132.1 2.9 %copy.37 = bf16[4,4,128,1152]{3,2,1,0:T(8,128)(2,1)S(1)} copy(bf16[4,4,128,1152]{3,2,0,1:T(8,128)(2,1)} %bitcast.37) | data formatting | bytes 9437184 | tf_op jit(solution)/shard_map/transpose | solution.py:435
  135.0 0.6 copy-done
  135.7 3.9 %fusion = f32[1024,768]{1,0:T(8,128)S(1)} fusion(bf16[1024,2048]{0,1:T(8,128)(2,1)S(1)} %bitcast.36, f32[2048]{0:T(1024)S(1)} %copy-done.8, f32[1024]{0:T(1024)S(1)} %add_rsqrt_fusion, bf16[2048,1152]{1,0:T(8,128)(2,1)S(1)} %bitcast.38), kind=kOutput, calls=%fused_computation.2 | convolution fusion | flops 3229614080 | bytes 10498048 | tf_op jit(solution)/shard_map/dot_general | solution.py:460
  139.6 0.5 fusion.5
  140.0 1.3 convolution_convert_fusion
  141.3 1.3 convolution_convert_fusion.1
  142.6 2.3 %pad_maximum_fusion.terms_ref = bf16[2,4,256,1024]{3,2,1,0:T(8,128)(2,1)} fusion(bf16[1,4,256,1024]{3,2,1,0:T(8,128)(2,1)S(1)} %bitcast.42, bf16[1,4,256,1024]{3,2,1,0:T(8,128)(2,1)S(1)} %bitcast.43), kind=kLoop, calls=%fused_computation.3 | loop fusion | flops 2097152 | bytes 8388608 | tf_op jit(solution)/shard_map/concatenate | solution.py:464
  144.9 32.2 %shard_map.161 = bf16[4,256,1024]{2,1,0:T(8,128)(2,1)} custom-call(bf16[2,4,256,1024]{3,2,1,0:T(8,128)(2,1)} %pad_maximum_fusion.terms_ref), custom_call_target="tpu_custom_call" | custom-call | flops 1000000000 | bytes 20000000 | tf_op jit(solution)/shard_map/pallas_call | solution.py:339
  177.2 2.1 %convert_reduce_fusion = f32[256,1024]{1,0:T(8,128)S(1)} fusion(bf16[4,256,1024]{2,1,0:T(8,128)(2,1)} %shard_map.161), kind=kLoop, calls=%fused_computation.4 | loop fusion | flops 1835008 | bytes 3145728 | tf_op jit(solution)/shard_map/reduce_sum | solution.py:476
  179.3 1.0 fusion.10
  (26 shorter events, 0.2 us)
Async XLA Ops:
  6.5 125.5 %all-gather.3.cloned.1.call-start = ((), (), s32[]{:S(2)}) async-start(), calls=%async_computation | async-start | bytes 5898240 | tf_op jit(solution)/shard_map/all_gather | solution.py:434
  15.8 25.8 %copy-start.2 = (f32[1408]{0:T(1024)S(1)}, f32[1408]{0:T(1024)}, u32[]{:S(2)}) copy-start(f32[1408]{0:T(1024)} %param.27) | copy-start | bytes 16900
  15.8 25.9 %copy-start.3 = (f32[1408]{0:T(1024)S(1)}, f32[1408]{0:T(1024)}, u32[]{:S(2)}) copy-start(f32[1408]{0:T(1024)} %param.29) | copy-start | bytes 16900
  15.8 26.0 %copy-start.6 = (f32[1,256,4]{1,2,0:T(4,128)S(1)}, f32[1,256,4]{1,2,0:T(4,128)}, u32[]{:S(2)}) copy-start(f32[1,256,4]{1,2,0:T(4,128)} %param.21) | copy-start | bytes 12292
  15.9 26.8 %copy-start.4 = (f32[2,1,1024]{2,1,0:T(1,128)S(1)}, f32[2,1,1024]{2,1,0:T(1,128)}, u32[]{:S(2)}) copy-start(f32[2,1,1024]{2,1,0:T(1,128)} %get-tuple-element.11) | copy-start | bytes 24580
  42.7 29.0 %copy-start.7 = (f32[512,1024]{1,0:T(8,128)S(1)}, f32[512,1024]{1,0:T(8,128)}, u32[]{:S(2)}) copy-start(f32[512,1024]{1,0:T(8,128)} %param.23) | copy-start | bytes 6291460
  76.0 7.4 %copy-start.1 = (bf16[4,256,256]{2,1,0:T(8,128)(2,1)S(1)}, bf16[4,256,256]{2,1,0:T(8,128)(2,1)}, u32[]{:S(2)}) copy-start(bf16[4,256,256]{2,1,0:T(8,128)(2,1)} %get-tuple-element.10) | copy-start | bytes 1572868
  132.1 3.6 %copy-start = (bf16[1024,4,2,256]{0,3,2,1:T(8,128)(2,1)S(1)}, bf16[1024,4,2,256]{0,3,2,1:T(8,128)(2,1)}, u32[]{:S(2)}) copy-start(bf16[1024,4,2,256]{0,3,2,1:T(8,128)(2,1)} %copy.35) | copy-start | bytes 12582916
  132.1 3.6 %copy-start.8 = (f32[2048]{0:T(1024)S(1)}, f32[2048]{0:T(1024)}, u32[]{:S(2)}) copy-start(f32[2048]{0:T(1024)} %param.25) | copy-start | bytes 24580
  177.2 2.1 %copy-start.5 = (f32[1024]{0:T(1024)S(1)}, f32[1024]{0:T(1024)}, u32[]{:S(2)}) copy-start(f32[1024]{0:T(1024)} %param.31) | copy-start | bytes 12292
Sparse Core Ops, SparseCore 0:
  41.7 90.3 all-gather.2
where the time goes:
time: 188 us; the launch traced here: 187 us
  Pallas kernels  124 us (66%)
  local copies, waits for them, and re-layouts  16.1 us (9%)
  between operations  13.7 us (7%)
  waiting for transfers between devices  12.5 us (7%)
  other arithmetic  11.4 us (6%)
  matrix products  9.31 us (5%)
    pallas_call x2, Pallas kernels, gather(): pl.pallas_call(functools.partial(gather_kernel, share), out_shape=jax.Sha...  45.4 us
    pallas_call x3, Pallas kernels, exchange(): pl.pallas_call(functools.partial(exchange_kernel, axis, n, spread, count)...  35.5 us
    pallas_call x1, Pallas kernels, reduce_back(): pl.pallas_call(functools.partial(reduce_kernel, n_fs), out_shape=jax.Shap...  32.2 us
    all_gather x1, waiting for transfers between devices, moving_body(): all_weights = lax.all_gather(got_weights, 'rep', axis=0, tiled=False)  12.5 us
    pallas_call x1, Pallas kernels, linear_attend(): pl.pallas_call(functools.partial(attend_kernel, head_total), out_shape=ja...  8.23 us
    transpose x1, local copies, waits for them, and re-layouts, moving_body(): updated = jnp.transpose(everywhere, (2, 1, 0, 3)).reshape(group_rows, width)  6.31 us
    dot_general x3, matrix products, by_rows(): lax.dot_general(left, right, (((1,), (1,)), ((), ())), preferred_element_...  5.45 us
    dot_general x1, matrix products, moving_body(): jnp.dot(normin, all_weights[:, :2 * padded], preferred_element_type=jnp.f...  3.87 us
  transfers between devices with their start and end apart: 1, of which 1 were waited for; matrix products, arithmetic and copies ran while one was open for 10% of the time, Pallas kernels for 32%

commit v1 on v0

v1 whole, which is shorter than its diff:
```python
import functools

import jax
import jax.numpy as jnp
from jax import lax
from jax.experimental import pallas as pl
from jax.experimental.pallas import tpu as pltpu
from jax.sharding import PartitionSpec as P

BLOCK = 64


epsilon = 1e-06
softness_factor = 16.0
highest = lax.Precision.HIGHEST


def attend_head(q, k, v, logodds, surge, gain):
    tokens, width = q.shape
    blocks = tokens // BLOCK
    mid = BLOCK // 2 - 1
    decay = (
        jnp.minimum(logodds, 0.0) - jnp.log1p(jnp.exp(-jnp.abs(logodds)))
    ) * (1.0 / softness_factor) + surge
    row = lax.broadcasted_iota(jnp.int32, (BLOCK, BLOCK), 0)
    col = lax.broadcasted_iota(jnp.int32, (BLOCK, BLOCK), 1)
    tri = jnp.where(row >= col, 1.0, 0.0).astype(jnp.bfloat16)
    q = q.astype(jnp.float32) * width ** (-0.5)
    k = k.astype(jnp.float32)
    high = decay.astype(jnp.bfloat16)
    low = (decay - high.astype(jnp.float32)).astype(jnp.bfloat16)
    pieces = []
    for n in range(blocks):
        rows = slice(n * BLOCK, (n + 1) * BLOCK)
        running = jnp.dot(tri, high[rows], preferred_element_type=jnp.float32) + jnp.dot(
            tri, low[rows], preferred_element_type=jnp.float32
        )
        before = running - decay[rows]
        center = running[mid : mid + 1]
        end = running[BLOCK - 1 : BLOCK]
        to_center = jnp.exp(center)
        from_center = jnp.exp(end - center)
        q_forward = q[rows] * jnp.exp(running - center)
        k_forward = k[rows] * jnp.exp(center - running)
        q_backward = q[rows] * jnp.exp(center - before)
        k_backward = k[rows] * jnp.exp(before - center)
        half = jnp.bfloat16
        scores = jnp.where(
            row >= col, by_rows(q_forward.astype(half), k_forward.astype(half)), 0.0
        ) + jnp.where(row <= col, by_rows(q_backward.astype(half), k_backward.astype(half)), 0.0)
        inner = jnp.dot(scores.astype(half), v[rows], preferred_element_type=jnp.float32)
        pieces.append(
            (
                inner,
                (q_forward * to_center).astype(half),
                (q_backward * from_center).astype(half),
                by_columns(v[rows], (k_forward * from_center).astype(half)),
                by_columns(v[rows], (k_backward * to_center).astype(half)),
                jnp.exp(end),
            )
        )
    totals = [piece[0] for piece in pieces]
    state = None
    for n in range(blocks):
        if state is not None:
            totals[n] = totals[n] + by_rows(pieces[n][1], state.astype(jnp.bfloat16))
        state = pieces[n][3] if state is None else pieces[n][5] * state + pieces[n][3]
    state = None
    for n in reversed(range(blocks)):
        if state is not None:
            totals[n] = totals[n] + by_rows(pieces[n][2], state.astype(jnp.bfloat16))
        state = pieces[n][4] if state is None else pieces[n][5] * state + pieces[n][4]
    attended = jnp.concatenate(totals, axis=0)
    scale = lax.rsqrt(jnp.mean(attended * attended, axis=-1, keepdims=True) + epsilon)
    return (attended * scale * gain).astype(jnp.bfloat16)


def by_columns(left, right):
    return lax.dot_general(
        left, right, (((0,), (0,)), ((), ())), preferred_element_type=jnp.float32
    )


def attend_kernel(head_total, q_ref, k_ref, v_ref, lo_ref, sg_ref, gain_ref, out_ref):
    width = q_ref.shape[1] // head_total
    value_width = v_ref.shape[1] // head_total
    for h in range(head_total):
        keys = slice(h * width, (h + 1) * width)
        values = slice(h * value_width, (h + 1) * value_width)
        out_ref[:, values] = attend_head(
            q_ref[:, keys],
            k_ref[:, keys],
            v_ref[:, values],
            lo_ref[:, keys],
            sg_ref[:, h : h + 1],
            gain_ref[...],
        )


def linear_attend(queries, key_matrix, value_matrix, decay_logodds, decay_surge, head_norm_gain):
    _, token_length, head_total = decay_surge.shape
    outs = [
        pl.pallas_call(
            functools.partial(attend_kernel, head_total),
            out_shape=jax.ShapeDtypeStruct(value_matrix.shape[1:], jnp.bfloat16),
            in_specs=[pl.BlockSpec(memory_space=pltpu.VMEM)] * 6,
            out_specs=pl.BlockSpec(memory_space=pltpu.VMEM),
            cost_estimate=pl.CostEstimate(
                flops=10**9, bytes_accessed=4 * 10**6, transcendentals=10**6
            ),
        )(
            queries[b], key_matrix[b], value_matrix[b], decay_logodds[b], decay_surge[b],
            head_norm_gain.reshape(1, -1),
        )
        for b in range(queries.shape[0])
    ]
    return jnp.concatenate(outs, axis=0)


def by_rows(left, right):
    return lax.dot_general(
        left, right, (((1,), (1,)), ((), ())), preferred_element_type=jnp.float32
    )


def body(
    residual,
    queries,
    key_matrix,
    value_matrix,
    decay_logodds,
    decay_surge,
    head_norm_gain,
    output_matrix,
    output_column_scale,
    premix_norm_gain,
    gate_matrix,
    gate_column_scale,
    up_matrix,
    up_column_scale,
    down_matrix,
    down_column_scale,
):
    sequence_batch, token_length, local_width = residual.shape
    row_count = sequence_batch * token_length
    normalized_rows = linear_attend(
        queries, key_matrix, value_matrix, decay_logodds, decay_surge, head_norm_gain
    )
    out_half = output_matrix.astype(jnp.bfloat16)
    out_full = lax.all_gather(out_half, "fs", axis=0, tiled=True)
    mix_terms = by_rows(normalized_rows, out_full)
    mix_total = lax.psum_scatter(
        mix_terms.astype(jnp.bfloat16), "tp", scatter_dimension=1, tiled=True
    ).astype(jnp.float32)
    own_rows = residual.reshape(row_count, local_width).astype(jnp.float32)
    updated = (own_rows + output_column_scale * mix_total).astype(jnp.bfloat16)
    features = lax.all_gather(updated, "tp", axis=1, tiled=True)
    wide_rows = features.astype(jnp.float32)
    factor = lax.rsqrt(jnp.mean(wide_rows * wide_rows, axis=-1, keepdims=True) + epsilon)
    normin = (wide_rows * factor * premix_norm_gain).astype(jnp.bfloat16)
    gate_half = gate_matrix.astype(jnp.bfloat16)
    up_half = up_matrix.astype(jnp.bfloat16)
    down_half = down_matrix.astype(jnp.bfloat16)
    gate_full, up_full, down_full = (
        lax.all_gather(gate_half, "fs", axis=0, tiled=True),
        lax.all_gather(up_half, "fs", axis=0, tiled=True),
        lax.all_gather(down_half, "fs", axis=0, tiled=True),
    )
    gate_pre = jnp.dot(normin, gate_full, preferred_element_type=jnp.float32)
    up_pre = jnp.dot(normin, up_full, preferred_element_type=jnp.float32)
    hidden = (jax.nn.silu(gate_pre * gate_column_scale) * (up_pre * up_column_scale)).astype(
        jnp.bfloat16
    )
    down_terms = by_rows(hidden, down_full)
    down_total = lax.psum_scatter(
        down_terms.astype(jnp.bfloat16), "tp", scatter_dimension=1, tiled=True
    ).astype(jnp.float32)
    result = (updated.astype(jnp.float32) + down_column_scale * down_total).astype(jnp.bfloat16)
    return result.reshape(sequence_batch, token_length, local_width)


def layer_kernel(
    q_hbm, k_hbm, v_hbm, lo_hbm, res_hbm, wo_hbm, gate_hbm, up_hbm, down_hbm,
    sg_ref, head_gain_ref, mlp_gain_ref, os_ref, gs_ref, us_ref, ds_ref,
    out_ref,
    q_v, k_v, v_v, lo_v, res_v, wo_f32, wo_half, wo_all,
    stage, own_f32, own_half, blocks, weights,
    normed, gathered, own_res, updated,
    os_all, gs_all, us_all, ds_all,
    own_down, to_p, to_p2, to_q, from_p, from_p2, from_q, result,
    load_sem, send_sem, recv_sem,
):
    r, f, t = lax.axis_index("rep"), lax.axis_index("fs"), lax.axis_index("tp")
    half = jnp.bfloat16
    x, y, c = f + 1 - 2 * lax.rem(f, 2), lax.rem(f + 2, 4), 3 - f
    p, q = x + t * (y - x), y + t * (x - y)
    fs_of = (f, x, y, c)
    m = lax.rem(r, 3)
    others = (lax.rem(m + 1, 3), lax.rem(m + 2, 3))
    mats = (gate_hbm, up_hbm, down_hbm)
    tokens, local_width = res_v.shape
    rows = tokens // 2
    own_width, total_units = stage.shape
    units = blocks.shape[2]
    part_rows = own_width // 2
    width = updated.shape[2]
    heads = sg_ref.shape[1]
    head_width = local_width // heads
    starts = [min(j * units, total_units - units) for j in range(4)]

    def lanes(start, size):
        return pl.ds(pl.multiple_of(start, 128), size)

    own_start = jnp.minimum(f * units, total_units - units)
    own_spill = f * units - own_start
    own_lanes = lanes(own_start, units)

    A, RES, CO, CX, CC = 0, 6, 10, 14, 30
    WO, SC, EP, EQ, EC, ZN, DN, FP, OUT = 38, 39, 43, 47, 51, 55, 73, 97, 103

    local_count = [0]
    waits = []

    def load(source, target):
        index = local_count[0]
        local_count[0] += 1
        copy = pltpu.make_async_copy(source, target, load_sem.at[index])
        return copy

    send_count = [0]
    sent = []

    def send(source, target, slot, device, when=None):
        index = send_count[0]
        send_count[0] += 1
        copy = pltpu.make_async_remote_copy(
            src_ref=source,
            dst_ref=target,
            send_sem=send_sem.at[index],
            recv_sem=recv_sem.at[slot],
            device_id=device,
            device_id_type=pl.DeviceIdType.MESH,
        )
        if when is None:
            copy.start()
        else:
            pl.when(when)(copy.start)
        sent.append((copy, when))

    def arrive(target, slot):
        pltpu.make_async_remote_copy(
            src_ref=target,
            dst_ref=target,
            send_sem=send_sem.at[0],
            recv_sem=recv_sem.at[slot],
            device_id=(r, f, 1 - t),
            device_id_type=pl.DeviceIdType.MESH,
        ).wait_recv()

    def part(n):
        return pl.ds(n * part_rows, part_rows)

    stage_loads = []
    for n in range(2):
        index = local_count[0]
        local_count[0] += 1
        for mm in range(3):
            @pl.when(m == mm)
            def _(mm=mm, n=n, index=index):
                pltpu.make_async_copy(
                    mats[mm].at[part(n)], stage.at[part(n)], load_sem.at[index]
                ).start()
        stage_loads.append(
            pltpu.make_async_copy(gate_hbm.at[part(n)], stage.at[part(n)], load_sem.at[index])
        )
    res_load = load(res_hbm, res_v)
    res_load.start()
    head_loads = []
    for h in range(heads):
        keys = slice(h * head_width, (h + 1) * head_width)
        loads = [
            load(a.at[:, keys], b.at[:, keys])
            for a, b in ((lo_hbm, lo_v), (q_hbm, q_v), (k_hbm, k_v), (v_hbm, v_v))
        ]
        for copy in loads:
            copy.start()
        head_loads.append(loads)
    wo_load = load(wo_hbm, wo_f32)
    wo_load.start()
    own_loads = []
    for n in range(2):
        index = local_count[0]
        local_count[0] += 1
        for mm in range(3):
            @pl.when(m == mm)
            def _(mm=mm, n=n, index=index):
                pltpu.make_async_copy(
                    mats[(mm + 1 + n) % 3].at[:, own_lanes], own_f32.at[n], load_sem.at[index]
                ).start()
        own_loads.append(
            pltpu.make_async_copy(gate_hbm.at[:, own_lanes], own_f32.at[n], load_sem.at[index])
        )

    partner = (r, f, 1 - t)
    peers = [partner]
    for other in (x, y, c):
        peers += [(r, other, 0), (r, other, 1)]
    peers += [(lax.rem(r + step, 4), f, t) for step in range(1, 4)]
    greet(peers)

    def weight_at(matrix, owner, n, core):
        return weights.at[
            matrix,
            pl.ds(owner * own_width + n * part_rows, part_rows),
            lanes(core * units, units),
        ]

    lane = lax.broadcasted_iota(jnp.int32, (part_rows, units), 1)
    for n in range(2):
        stage_loads[n].wait()
        span = slice(n * part_rows, (n + 1) * part_rows)
        for j in range(4):
            cut = stage[span, starts[j] : starts[j] + units]
            spill = j * units - starts[j]
            if spill > 0:
                cut = jnp.where((lane < spill) & (m == 2), 0.0, cut)
            blocks[j, span, :] = cut.astype(half)
        for rel in (1, 2, 3):
            send(
                blocks.at[fs_of[rel], part(n)], weight_at(m, f, n, t), A + n * 3 + rel - 1,
                (r, fs_of[rel], t),
            )
    own_copies = []
    for n in range(2):
        copy = load(blocks.at[f, part(n)], weight_at(m, f, n, t))
        copy.start()
        own_copies.append(copy)
        send(blocks.at[f, part(n)], weight_at(m, f, n, t), DN + m * 8 + n, partner)

    for n, (ref, both) in enumerate(
        ((os_ref, os_all), (gs_ref, gs_all), (us_ref, us_all), (ds_ref, ds_all))
    ):
        both[t] = ref[...]
        send(ref, both.at[t], SC + n, partner)

    res_load.wait()
    mine = jnp.where(lax.div(f, 2) == t, 1, 0)
    first = mine * x + (1 - mine) * c
    second = mine * f + (1 - mine) * y
    first_slot = RES + mine + (1 - mine) * 3
    second_slot = RES + (1 - mine) * 2
    target = own_res.at[f]
    for core in range(2):
        send(
            res_v.at[pl.ds(core * rows, rows), lanes((first - 2 * t) * own_width, own_width)],
            target, first_slot, (r, first, core),
        )
    second_lanes = lanes((second - 2 * t) * own_width, own_width)
    send(res_v.at[pl.ds((1 - t) * rows, rows), second_lanes], target, second_slot, (r, second, 1 - t))
    send(
        res_v.at[pl.ds(t * rows, rows), second_lanes], target, second_slot, (r, second, t),
        when=mine == 0,
    )
    kept_res = pltpu.make_async_copy(
        res_v.at[pl.ds(t * rows, rows), second_lanes], target, recv_sem.at[RES]
    )
    pl.when(mine == 1)(kept_res.start)

    def head_lanes(core, h):
        return lanes((core * heads + h) * head_width, head_width)

    def pump(n, rel):
        block = weight_at(m, fs_of[rel], n, t)
        arrive(block, A + n * 3 + rel - 1)
        send(block, block, DN + m * 8 + rel * 2 + n, partner)

    def along_z(n, rel, late):
        block = weight_at(m, fs_of[rel], n, t)
        for step in range(1, 4):
            to = lax.rem(r + step, 4)
            near = (to - r == 1) | (r - to == 1)
            if late:
                when = r == 2
            else:
                when = (r == 1) | (near & (r != 2))
            send(block, block, ZN + m * 6 + n * 3 + rel - 1, (to, f, t), when=when)

    for h in range(heads):
        keys = slice(h * head_width, (h + 1) * head_width)
        for copy in head_loads[h]:
            copy.wait()
        normed[h] = attend_head(
            q_v[:, keys], k_v[:, keys], v_v[:, keys], lo_v[:, keys],
            sg_ref[:, h : h + 1], head_gain_ref[...],
        )
        target = gathered.at[f, :, head_lanes(t, h)]
        for to, slot in ((x, CX), (y, CX + 8)):
            for core in range(2):
                send(
                    normed.at[h, pl.ds(core * rows, rows)], target, slot + t * 4 + h,
                    (r, to, core),
                )
        send(normed.at[h, pl.ds((1 - t) * rows, rows)], target, CO + h, partner)
        copy = load(normed.at[h, pl.ds(t * rows, rows)], target)
        copy.start()
        own_copies.append(copy)

    for rel in (1, 2):
        pump(0, rel)
        along_z(0, rel, False)

    wo_load.wait()
    wo_half[...] = wo_f32[...].astype(half)
    target = wo_all.at[:, lanes(t * local_width, local_width)]
    send(wo_half, target, WO, partner)
    copy = load(wo_half, target)
    copy.start()
    own_copies.append(copy)
    own_lane = lax.broadcasted_iota(jnp.int32, (own_width, units), 1)
    for n in range(2):
        own_loads[n].wait()
        cut = jnp.where((own_lane < own_spill) & (others[n] == 2), 0.0, own_f32[n])
        own_half[n] = cut.astype(half)
        target = weights.at[
            others[n], pl.ds(f * own_width, own_width), lanes(t * units, units)
        ]
        send(own_half.at[n], target, DN + others[n] * 8, partner)
        copy = load(own_half.at[n], target)
        copy.start()
        own_copies.append(copy)

    for n, rel in ((0, 3), (1, 1), (1, 2), (1, 3)):
        pump(n, rel)
        along_z(n, rel, False)

    from_p_slot, from_q_slot = CX + 8 * t, CX + 8 * (1 - t)
    for h in range(heads):
        for core in range(2):
            block = gathered.at[p, :, head_lanes(core, h)]
            arrive(block, from_p_slot + core * 4 + h)
            send(block, block, CC + core * 4 + h, (r, q, t))

    for n in range(2):
        for rel in (1, 2, 3):
            along_z(n, rel, True)

    for copy in own_copies:
        copy.wait()
    for n, both in enumerate((os_all, gs_all, us_all, ds_all)):
        arrive(both.at[1 - t], SC + n)
    arrive(wo_all.at[:, lanes((1 - t) * local_width, local_width)], WO)
    out_scale = os_all[lax.div(f, 2), :, lanes(lax.rem(f, 2) * own_width, own_width)]
    order = (f, p, q, c)
    res_slots = (RES, RES + 1 + t, RES + 2 - t, RES + 3)

    def feature_lanes(owner):
        return lanes(owner * own_width, own_width)

    for k in range(4):
        seq = order[k]
        if k == 0:
            for h in range(heads):
                arrive(gathered.at[f, :, head_lanes(1 - t, h)], CO + h)
        elif k > 1:
            slot = from_q_slot if k == 2 else CC
            for h in range(heads):
                for core in range(2):
                    arrive(gathered.at[seq, :, head_lanes(core, h)], slot + core * 4 + h)
        arrive(own_res.at[seq], res_slots[k])
        mixed = by_rows(gathered[seq], wo_all[...])
        updated[seq, :, feature_lanes(f)] = (
            own_res[seq].astype(jnp.float32) + out_scale * mixed
        ).astype(half)
        block = updated.at[seq, :, feature_lanes(f)]
        send(block, block, EP + (k ^ 1), (r, p, t))
        send(block, block, EQ + (k ^ 2), (r, q, t))

    def pump_z(matrix):
        for n in range(2):
            for rel in (1, 2, 3):
                block = weight_at(matrix, fs_of[rel], n, t)
                arrive(block, ZN + matrix * 6 + n * 3 + rel - 1)
                send(block, block, DN + matrix * 8 + rel * 2 + n, partner)

    zero, two = jnp.where(m == 0, 1, 0), jnp.where(m == 2, 1, 0)
    pump_z(zero)
    for k in range(4):
        block = updated.at[order[k], :, feature_lanes(p)]
        arrive(block, EP + k)
        send(block, block, EC + (k ^ 2), (r, q, t))
    pump_z(2 - two)

    arrive_whole = [
        weights.at[
            others[n], pl.ds(f * own_width, own_width), lanes((1 - t) * units, units)
        ]
        for n in range(2)
    ]
    for n in range(2):
        arrive(arrive_whole[n], DN + others[n] * 8)
        arrive(weight_at(m, f, n, 1 - t), DN + m * 8 + n)
    for matrix in range(3):
        for rel in (1, 2, 3):
            for n in range(2):
                arrive(
                    weight_at(matrix, fs_of[rel], n, 1 - t), DN + matrix * 8 + rel * 2 + n
                )

    gate_scale = jnp.concatenate([gs_all[0, :, own_lanes], gs_all[1, :, own_lanes]], axis=1)
    up_scale = jnp.concatenate([us_all[0, :, own_lanes], us_all[1, :, own_lanes]], axis=1)
    columns = width // 2

    def piece(n):
        return slice(n * columns, (n + 1) * columns)

    for k in (3, 1, 0, 2):
        seq = order[k]
        arrive(updated.at[seq, :, feature_lanes(q)], EQ + k)
        arrive(updated.at[seq, :, feature_lanes(c)], EC + k)
        wide = updated[seq].astype(jnp.float32)
        factor = lax.rsqrt(jnp.mean(wide * wide, axis=-1, keepdims=True) + epsilon)
        normin = (wide * factor * mlp_gain_ref[...]).astype(half)
        gate_pre = jnp.dot(normin, weights[0], preferred_element_type=jnp.float32) * gate_scale
        up_pre = jnp.dot(normin, weights[1], preferred_element_type=jnp.float32) * up_scale
        hidden = (jax.nn.silu(gate_pre) * up_pre).astype(half)
        for n in range(2):
            term = by_rows(hidden, weights[2, piece(n), :])
            if k == 3:
                to_p[:, piece(n)] = term.astype(half)
                send(to_p.at[:, piece(n)], from_p.at[:, piece(n)], FP + n, (r, p, t))
            elif k == 1:
                to_p2[:, piece(n)] = term.astype(half)
                send(to_p2.at[:, piece(n)], from_p2.at[:, piece(n)], FP + 2 + n, (r, p, t))
            elif k == 0:
                own_down[:, piece(n)] = term
            else:
                arrive(from_p.at[:, piece(n)], FP + n)
                total = term + from_p[:, piece(n)].astype(jnp.float32)
                to_q[:, piece(n)] = total.astype(half)
                send(to_q.at[:, piece(n)], from_q.at[:, piece(n)], FP + 4 + n, (r, q, t))

    down_scale = jnp.concatenate([ds_all[0], ds_all[1]], axis=1)
    for n in range(2):
        arrive(from_p2.at[:, piece(n)], FP + 2 + n)
        own_down[:, piece(n)] += from_p2[:, piece(n)].astype(jnp.float32)
    for n in range(2):
        arrive(from_q.at[:, piece(n)], FP + 4 + n)
        total = own_down[:, piece(n)] + from_q[:, piece(n)].astype(jnp.float32)
        result[:, piece(n)] = (
            updated[f, :, piece(n)].astype(jnp.float32) + down_scale[:, piece(n)] * total
        ).astype(half)
    mine_rows = pl.ds(t * rows, rows)
    send(
        result.at[:, lanes((1 - t) * local_width, local_width)], out_ref.at[mine_rows], OUT, partner
    )
    out_ref[mine_rows, :] = result[:, lanes(t * local_width, local_width)]
    arrive(out_ref.at[pl.ds((1 - t) * rows, rows)], OUT)
    for copy, when in sent:
        if when is None:
            copy.wait_send()
        else:
            pl.when(when)(copy.wait_send)


def one_kernel_body(
    sizes,
    residual,
    queries,
    key_matrix,
    value_matrix,
    decay_logodds,
    decay_surge,
    head_norm_gain,
    output_matrix,
    output_column_scale,
    premix_norm_gain,
    gate_matrix,
    gate_column_scale,
    up_matrix,
    up_column_scale,
    down_matrix,
    down_column_scale,
):
    half, full = jnp.bfloat16, jnp.float32
    _, tokens, local_width = residual.shape
    rows = tokens // 2
    own_width, total_units = gate_matrix.shape
    width = premix_norm_gain.shape[0]
    heads = decay_surge.shape[2]
    units = -(-total_units // (128 * 4)) * 128
    hbm, vmem = pl.BlockSpec(memory_space=pl.ANY), pl.BlockSpec(memory_space=pltpu.VMEM)
    out = pl.pallas_call(
        layer_kernel,
        out_shape=jax.ShapeDtypeStruct((tokens, local_width), half),
        in_specs=[hbm] * 9 + [vmem] * 7,
        out_specs=vmem,
        scratch_shapes=[
            pltpu.VMEM((tokens, local_width), half),
            pltpu.VMEM((tokens, local_width), half),
            pltpu.VMEM((tokens, local_width), half),
            pltpu.VMEM((tokens, local_width), full),
            pltpu.VMEM((tokens, local_width), half),
            pltpu.VMEM((own_width, local_width), full),
            pltpu.VMEM((own_width, local_width), half),
            pltpu.VMEM((own_width, width), half),
            pltpu.VMEM((own_width, total_units), full),
            pltpu.VMEM((2, own_width, units), full),
            pltpu.VMEM((2, own_width, units), half),
            pltpu.VMEM((4, own_width, units), half),
            pltpu.VMEM((3, width, 2 * units), half),
            pltpu.VMEM((heads, tokens, local_width // heads), half),
            pltpu.VMEM((4, rows, width), half),
            pltpu.VMEM((4, rows, own_width), half),
            pltpu.VMEM((4, rows, width), half),
            pltpu.VMEM((2, 1, local_width), full),
            pltpu.VMEM((2, 1, total_units), full),
            pltpu.VMEM((2, 1, total_units), full),
            pltpu.VMEM((2, 1, local_width), full),
            pltpu.VMEM((rows, width), full),
        ]
        + [pltpu.VMEM((rows, width), half)] * 7
        + [
            pltpu.SemaphoreType.DMA((64,)),
            pltpu.SemaphoreType.DMA((160,)),
            pltpu.SemaphoreType.DMA((104,)),
        ],
        compiler_params=pltpu.CompilerParams(
            collective_id=1, has_side_effects=True, vmem_limit_bytes=60 * 2**20
        ),
    )(
        queries[0], key_matrix[0], value_matrix[0], decay_logodds[0], residual[0],
        output_matrix, gate_matrix, up_matrix, down_matrix,
        decay_surge[0], head_norm_gain.reshape(1, -1), premix_norm_gain.reshape(1, -1),
        output_column_scale.reshape(1, -1), gate_column_scale.reshape(1, -1),
        up_column_scale.reshape(1, -1), down_column_scale.reshape(1, -1),
    )
    return out[None]


def greet(devices):
    barrier = pltpu.get_barrier_semaphore()
    for device in devices:
        pl.semaphore_signal(
            barrier, inc=1, device_id=device, device_id_type=pl.DeviceIdType.MESH
        )
    pl.semaphore_wait(barrier, len(devices))


def chosen_body(mesh):
    sizes = tuple(mesh.shape[name] for name in ("rep", "fs", "tp"))

    def run(*args):
        residual, surge, output_matrix, gate_matrix = args[0], args[5], args[7], args[10]
        sequences, tokens, local_width = residual.shape
        own_width, total_units = gate_matrix.shape
        fits = (
            sizes == (4, 4, 2)
            and sequences == 1
            and tokens % (2 * BLOCK) == 0
            and local_width == 2 * own_width
            and output_matrix.shape == (own_width, local_width)
            and own_width % 128 == 0
            and total_units % 128 == 0
            and total_units >= 512
            and (local_width // surge.shape[2]) % 128 == 0
            and surge.shape[2] == 4
        )
        if fits:
            return one_kernel_body(sizes, *args)
        return body(*args)

    return run


def solution(mesh):
    return jax.shard_map(
        chosen_body(mesh),
        mesh=mesh,
        in_specs=(
            P(("rep", "fs"), None, "tp"),
            P(("rep", "fs"), None, "tp"),
            P(("rep", "fs"), None, "tp"),
            P(("rep", "fs"), None, "tp"),
            P(("rep", "fs"), None, "tp"),
            P(("rep", "fs"), None, "tp"),
            P(),
            P("fs", "tp"),
            P("tp"),
            P(),
            P("fs", "tp"),
            P("tp"),
            P("fs", "tp"),
            P("tp"),
            P("fs", "tp"),
            P("tp"),
        ),
        out_specs=P(("rep", "fs"), None, "tp"),
        check_vma=False,
    )
```

time: 188 us -> 125 us (0.66)
  between operations: 13.7 us -> 0.01 us
  waiting for transfers between devices: 12.5 us -> 0 us
  other arithmetic: 11.4 us -> 0 us
  local copies, waits for them, and re-layouts: 16.1 us -> 5.93 us
  matrix products: 9.31 us -> 0 us
  Pallas kernels: 124 us -> 118 us
    all_gather x1 -> x0, waiting for transfers between devices: 12.5 us -> none  [moving_body(): all_weights = lax.all_gather(got_weights, 'rep', axis=0, tiled=False)]
    transpose x3 -> x0, local copies, waits for them, and re-layouts: 10.7 us -> none  [the longest x1 6.31 us: moving_body(): updated = jnp.transpose(everywhere, (2, 1, 0, 3)).reshape(group_rows, width)]
    dot_general x4 -> x0, matrix products: 9.31 us -> none  [the longest x3 5.45 us: by_rows(): lax.dot_general(left, right, (((1,), (1,)), ((), ())), preferred_element_...]
    reduce_sum x3 -> x0, other arithmetic: 6.72 us -> none  [the longest x1 3.07 us: moving_body(): jnp.mean(wide_rows * wide_rows, axis=-1, keepdims=True) + epsilon]
    pallas_call x8 -> x1, Pallas kernels: 124 us -> 118 us  [one_kernel_body(): pl.pallas_call(layer_kernel, out_shape=jax.ShapeDtypeStruct((tokens, loca...]
    concatenate x1 -> x0, other arithmetic: 2.29 us -> none  [moving_body(): jnp.concatenate([by_rows(hidden, all_weights[t * local_width:(t + 1) * lo...]
    dynamic_slice x5 -> x0, local copies, waits for them, and re-layouts: 2.16 us -> none  [the longest x1 1.08 us: moving_body(): lax.dynamic_slice(updated, (fs * row_count, tp * local_width), (row_count...]
  transfers between devices with their start and end apart: 1 -> 0, of which waited for: 1 -> 0; matrix products, arithmetic and copies ran while one was open for 10% -> 0% of each run, Pallas kernels for 32% -> 0%
where the time goes in v1:
time: 125 us; the launch traced here: 124 us
  Pallas kernels  118 us (94%)
  local copies, waits for them, and re-layouts  5.93 us (5%)
    pallas_call x1, Pallas kernels, one_kernel_body(): pl.pallas_call(layer_kernel, out_shape=jax.ShapeDtypeStruct((tokens, loca...  118 us
    unnamed x2, local copies, waits for them, and re-layouts  3.35 us

profile of v1, /device:TPU:1, one launch (start us, length us, event | category | flops | bytes accessed | tf_op | source)
XLA Modules:
  0.0 123.8 jit_solution(1984502743875980283)
XLA Ops:
  0.0 1.3 %reshape.21.gs_ref = f32[1,1408]{1,0:T(1,128)} reshape(f32[1408]{0:T(1024)} %param.27) | data formatting | bytes 11264 | tf_op jit(solution)/shard_map/reshape | solution.py:634
  1.3 1.3 %reshape.22.us_ref = f32[1,1408]{1,0:T(1,128)} reshape(f32[1408]{0:T(1024)} %param.29) | data formatting | bytes 11264 | tf_op jit(solution)/shard_map/reshape | solution.py:635
  2.6 1.5 %copy.17 = f32[1,256,4]{2,1,0:T(8,128)} copy(f32[1,256,4]{1,2,0:T(4,128)} %param.21) | data formatting | bytes 8192 | tf_op args[5]
  4.1 117.9 %shard_map.154 = bf16[256,1024]{1,0:T(8,128)(2,1)} custom-call(bf16[256,1024]{1,0:T(8,128)(2,1)} %bitcast.14, bf16[256,1024]{1,0:T(8,128)(2,1)} %bitcast.15, bf16[256,1024]{1,0:T(8,128)(2,1)} %bitcast.16, f32[256,1024]{1,0:T(8,128)} %bitcast.12, bf16[256,1024]{1,0:T(8,128)(2,1)} %bitcast.17, f32[512,1024]{1,0:T(8,128)} %wo_hbm.1, f32[512,1408]{1,0:T(8,128)} %gate_hbm.1, ...), custom_call_target="tpu_custom_call" | custom-call | tf_op jit(solution)/shard_map/pallas_call | solution.py:592
  122.0 1.9 %copy.19 = bf16[1,256,1024]{2,1,0:T(8,128)(2,1)} copy(bf16[1,256,1024]{2,1,0:T(8,128)(2,1)} %bitcast.11) | data formatting | bytes 1048576

commit v2 on v1

v2 whole, which is shorter than its diff:
```python
import functools

import jax
import jax.numpy as jnp
from jax import lax
from jax.experimental import pallas as pl
from jax.experimental.pallas import tpu as pltpu
from jax.sharding import PartitionSpec as P

BLOCK = 64


epsilon = 1e-06
softness_factor = 16.0
highest = lax.Precision.HIGHEST


def attend_head(q, k, v, logodds, surge, gain):
    tokens, width = q.shape
    blocks = tokens // BLOCK
    mid = BLOCK // 2 - 1
    decay = (
        jnp.minimum(logodds, 0.0) - jnp.log1p(jnp.exp(-jnp.abs(logodds)))
    ) * (1.0 / softness_factor) + surge
    row = lax.broadcasted_iota(jnp.int32, (BLOCK, BLOCK), 0)
    col = lax.broadcasted_iota(jnp.int32, (BLOCK, BLOCK), 1)
    tri = jnp.where(row >= col, 1.0, 0.0).astype(jnp.bfloat16)
    q = q.astype(jnp.float32) * width ** (-0.5)
    k = k.astype(jnp.float32)
    high = decay.astype(jnp.bfloat16)
    low = (decay - high.astype(jnp.float32)).astype(jnp.bfloat16)
    pieces = []
    for n in range(blocks):
        rows = slice(n * BLOCK, (n + 1) * BLOCK)
        running = jnp.dot(tri, high[rows], preferred_element_type=jnp.float32) + jnp.dot(
            tri, low[rows], preferred_element_type=jnp.float32
        )
        before = running - decay[rows]
        center = running[mid : mid + 1]
        end = running[BLOCK - 1 : BLOCK]
        to_center = jnp.exp(center)
        from_center = jnp.exp(end - center)
        q_forward = q[rows] * jnp.exp(running - center)
        k_forward = k[rows] * jnp.exp(center - running)
        q_backward = q[rows] * jnp.exp(center - before)
        k_backward = k[rows] * jnp.exp(before - center)
        half = jnp.bfloat16
        scores = jnp.where(
            row >= col, by_rows(q_forward.astype(half), k_forward.astype(half)), 0.0
        ) + jnp.where(row <= col, by_rows(q_backward.astype(half), k_backward.astype(half)), 0.0)
        inner = jnp.dot(scores.astype(half), v[rows], preferred_element_type=jnp.float32)
        pieces.append(
            (
                inner,
                (q_forward * to_center).astype(half),
                (q_backward * from_center).astype(half),
                by_columns(v[rows], (k_forward * from_center).astype(half)),
                by_columns(v[rows], (k_backward * to_center).astype(half)),
                jnp.exp(end),
            )
        )
    totals = [piece[0] for piece in pieces]
    state = None
    for n in range(blocks):
        if state is not None:
            totals[n] = totals[n] + by_rows(pieces[n][1], state.astype(jnp.bfloat16))
        state = pieces[n][3] if state is None else pieces[n][5] * state + pieces[n][3]
    state = None
    for n in reversed(range(blocks)):
        if state is not None:
            totals[n] = totals[n] + by_rows(pieces[n][2], state.astype(jnp.bfloat16))
        state = pieces[n][4] if state is None else pieces[n][5] * state + pieces[n][4]
    attended = jnp.concatenate(totals, axis=0)
    scale = lax.rsqrt(jnp.mean(attended * attended, axis=-1, keepdims=True) + epsilon)
    return (attended * scale * gain).astype(jnp.bfloat16)


def by_columns(left, right):
    return lax.dot_general(
        left, right, (((0,), (0,)), ((), ())), preferred_element_type=jnp.float32
    )


def attend_kernel(head_total, q_ref, k_ref, v_ref, lo_ref, sg_ref, gain_ref, out_ref):
    width = q_ref.shape[1] // head_total
    value_width = v_ref.shape[1] // head_total
    for h in range(head_total):
        keys = slice(h * width, (h + 1) * width)
        values = slice(h * value_width, (h + 1) * value_width)
        out_ref[:, values] = attend_head(
            q_ref[:, keys],
            k_ref[:, keys],
            v_ref[:, values],
            lo_ref[:, keys],
            sg_ref[:, h : h + 1],
            gain_ref[...],
        )


def linear_attend(queries, key_matrix, value_matrix, decay_logodds, decay_surge, head_norm_gain):
    _, token_length, head_total = decay_surge.shape
    outs = [
        pl.pallas_call(
            functools.partial(attend_kernel, head_total),
            out_shape=jax.ShapeDtypeStruct(value_matrix.shape[1:], jnp.bfloat16),
            in_specs=[pl.BlockSpec(memory_space=pltpu.VMEM)] * 6,
            out_specs=pl.BlockSpec(memory_space=pltpu.VMEM),
            cost_estimate=pl.CostEstimate(
                flops=10**9, bytes_accessed=4 * 10**6, transcendentals=10**6
            ),
        )(
            queries[b], key_matrix[b], value_matrix[b], decay_logodds[b], decay_surge[b],
            head_norm_gain.reshape(1, -1),
        )
        for b in range(queries.shape[0])
    ]
    return jnp.concatenate(outs, axis=0)


def by_rows(left, right):
    return lax.dot_general(
        left, right, (((1,), (1,)), ((), ())), preferred_element_type=jnp.float32
    )


def body(
    residual,
    queries,
    key_matrix,
    value_matrix,
    decay_logodds,
    decay_surge,
    head_norm_gain,
    output_matrix,
    output_column_scale,
    premix_norm_gain,
    gate_matrix,
    gate_column_scale,
    up_matrix,
    up_column_scale,
    down_matrix,
    down_column_scale,
):
    sequence_batch, token_length, local_width = residual.shape
    row_count = sequence_batch * token_length
    normalized_rows = linear_attend(
        queries, key_matrix, value_matrix, decay_logodds, decay_surge, head_norm_gain
    )
    out_half = output_matrix.astype(jnp.bfloat16)
    out_full = lax.all_gather(out_half, "fs", axis=0, tiled=True)
    mix_terms = by_rows(normalized_rows, out_full)
    mix_total = lax.psum_scatter(
        mix_terms.astype(jnp.bfloat16), "tp", scatter_dimension=1, tiled=True
    ).astype(jnp.float32)
    own_rows = residual.reshape(row_count, local_width).astype(jnp.float32)
    updated = (own_rows + output_column_scale * mix_total).astype(jnp.bfloat16)
    features = lax.all_gather(updated, "tp", axis=1, tiled=True)
    wide_rows = features.astype(jnp.float32)
    factor = lax.rsqrt(jnp.mean(wide_rows * wide_rows, axis=-1, keepdims=True) + epsilon)
    normin = (wide_rows * factor * premix_norm_gain).astype(jnp.bfloat16)
    gate_half = gate_matrix.astype(jnp.bfloat16)
    up_half = up_matrix.astype(jnp.bfloat16)
    down_half = down_matrix.astype(jnp.bfloat16)
    gate_full, up_full, down_full = (
        lax.all_gather(gate_half, "fs", axis=0, tiled=True),
        lax.all_gather(up_half, "fs", axis=0, tiled=True),
        lax.all_gather(down_half, "fs", axis=0, tiled=True),
    )
    gate_pre = jnp.dot(normin, gate_full, preferred_element_type=jnp.float32)
    up_pre = jnp.dot(normin, up_full, preferred_element_type=jnp.float32)
    hidden = (jax.nn.silu(gate_pre * gate_column_scale) * (up_pre * up_column_scale)).astype(
        jnp.bfloat16
    )
    down_terms = by_rows(hidden, down_full)
    down_total = lax.psum_scatter(
        down_terms.astype(jnp.bfloat16), "tp", scatter_dimension=1, tiled=True
    ).astype(jnp.float32)
    result = (updated.astype(jnp.float32) + down_column_scale * down_total).astype(jnp.bfloat16)
    return result.reshape(sequence_batch, token_length, local_width)


VMEM_MIB = 60
EARLY_PART = 4
EXTRA_PART = 8


def layer_kernel(
    q_hbm, k_hbm, v_hbm, lo_hbm, res_hbm, wo_hbm, gate_hbm, up_hbm, down_hbm,
    sg_ref, head_gain_ref, mlp_gain_ref, os_ref, gs_ref, us_ref, ds_ref,
    out_ref,
    q_v, k_v, v_v, lo_v, res_v, wo_f32, wo_half, wo_all,
    stage, own_f32, own_half, blocks, extra_stage, extra_blocks, weights,
    normed, gathered, own_res, updated, os_all, gs_all, us_all,
    own_down, other_down, other_updated, to_p, to_p2, to_q, from_p, from_p2, from_q,
    load_sem, send_sem, recv_sem,
):
    r, f, t = lax.axis_index("rep"), lax.axis_index("fs"), lax.axis_index("tp")
    half = jnp.bfloat16
    x, y, c = f + 1 - 2 * lax.rem(f, 2), lax.rem(f + 2, 4), 3 - f
    p, q = x + t * (y - x), y + t * (x - y)
    fs_of = (f, x, y, c)
    partner = (r, f, 1 - t)
    m = lax.rem(r, 3)
    zero, second = jnp.where(m == 0, 1, 0), jnp.where(m == 2, 1, 2)
    along = (zero, second)
    others = (lax.rem(m + 1, 3), lax.rem(m + 2, 3))
    mats = (gate_hbm, up_hbm, down_hbm)
    tokens, local_width = res_v.shape
    rows = tokens // 2
    own_width, total_units = stage.shape
    units = blocks.shape[2]
    width = updated.shape[2]
    heads = sg_ref.shape[0]
    head_width = local_width // heads
    starts = [min(j * units, total_units - units) for j in range(4)]
    early, extra = own_width // EARLY_PART, own_width // EXTRA_PART
    pieces = ((0, early), (early, own_width - early))
    kept = own_width - extra

    SA, SD, SS, SR, SX, SH, SZ, SWO, SC, SE, SF, SO = 0, 3, 4, 7, 11, 12, 15, 18, 19, 20, 23, 26
    A, RES, CP, CQ, CC, CO, WO, SCALE = 0, 6, 7, 15, 16, 17, 18, 19
    EP, EQ, EC, ZN, DN, XN, FP, OUT = 22, 26, 30, 34, 46, 47, 48, 54
    LSTAGE, LEXTRA, LRES, LHEAD, LWO, LOWN, LKEPT, LEND = 0, 2, 3, 4, 12, 13, 15, 18

    def lanes(start, size):
        return pl.ds(pl.multiple_of(start, 128), size)

    def part(n):
        return pl.ds(*pieces[n])

    def local(source, target, sem):
        return pltpu.make_async_copy(source, target, load_sem.at[sem])

    def send(source, target, sem, slot, device, when=None):
        copy = pltpu.make_async_remote_copy(
            src_ref=source,
            dst_ref=target,
            send_sem=send_sem.at[sem],
            recv_sem=recv_sem.at[slot],
            device_id=device,
            device_id_type=pl.DeviceIdType.MESH,
        )
        if when is None:
            copy.start()
        else:
            pl.when(when)(copy.start)

    def waiter(target, sem, slot):
        return pltpu.make_async_remote_copy(
            src_ref=target,
            dst_ref=target,
            send_sem=send_sem.at[sem],
            recv_sem=recv_sem.at[slot],
            device_id=partner,
            device_id_type=pl.DeviceIdType.MESH,
        )

    def arrive(target, slot):
        waiter(target, 0, slot).wait_recv()

    open_scope = []

    def phase(name):
        if open_scope:
            open_scope.pop().__exit__(None, None, None)
        if name:
            scope = jax.named_scope(name)
            scope.__enter__()
            open_scope.append(scope)

    phase("loads")
    own_start = jnp.minimum(f * units, total_units - units)
    own_spill = f * units - own_start
    own_lanes = lanes(own_start, units)
    extra_rows = pl.ds(kept, extra)
    for n in range(2):
        for mm in range(3):
            @pl.when(m == mm)
            def _(mm=mm, n=n):
                local(mats[mm].at[part(n)], stage.at[part(n)], LSTAGE + n).start()
    local(res_hbm, res_v, LRES).start()
    for mm in (1, 2):
        @pl.when(second == mm)
        def _(mm=mm):
            local(mats[mm].at[extra_rows], extra_stage, LEXTRA).start()
    for h in range(heads):
        keys = slice(h * head_width, (h + 1) * head_width)
        local(lo_hbm.at[:, keys], lo_v.at[:, keys], LHEAD + 2 * h).start()
        for a, b in ((q_hbm, q_v), (k_hbm, k_v), (v_hbm, v_v)):
            local(a.at[:, keys], b.at[:, keys], LHEAD + 2 * h + 1).start()
    local(wo_hbm, wo_f32, LWO).start()
    for n in range(2):
        for mm in range(3):
            @pl.when(m == mm)
            def _(mm=mm, n=n):
                local(
                    mats[(mm + 1 + n) % 3].at[:, own_lanes], own_f32.at[n], LOWN + n
                ).start()

    phase("greet")
    peers = [partner]
    for other in (x, y, c):
        peers += [(r, other, 0), (r, other, 1)]
    peers += [(lax.rem(r + step, 4), f, t) for step in range(1, 4)]
    greet(peers)

    def weight_rows(matrix, owner, start, size, core):
        return weights.at[
            matrix, pl.ds(owner * own_width + start, size), lanes(core * units, units)
        ]

    def weight_at(matrix, owner, n, size=None):
        return weight_rows(matrix, owner, pieces[n][0], size or pieces[n][1], t)

    def cut_blocks(source, target, start, size, matrix):
        lane = lax.broadcasted_iota(jnp.int32, (size, units), 1)
        span = slice(start, start + size)
        for j in range(4):
            cut = source[span, starts[j] : starts[j] + units]
            spill = j * units - starts[j]
            if spill > 0:
                cut = jnp.where((lane < spill) & (matrix == 2), 0.0, cut)
            target[j, span, :] = cut.astype(half)

    phase("cut_send")
    for n in range(2):
        local(gate_hbm.at[part(n)], stage.at[part(n)], LSTAGE + n).wait()
        cut_blocks(stage, blocks, *pieces[n], m)
        for rel in (1, 2, 3):
            send(
                blocks.at[fs_of[rel], part(n)], weight_at(m, f, n),
                SA + rel - 1, A + n * 3 + rel - 1, (r, fs_of[rel], t),
            )
    target = weight_rows(m, f, 0, own_width, t)
    local(blocks.at[f], target, LKEPT).start()
    send(blocks.at[f], target, SD, DN, partner)

    for n, (ref, both) in enumerate(((os_ref, os_all), (gs_ref, gs_all), (us_ref, us_all))):
        both[t] = ref[...].reshape(1, -1)
        send(both.at[t], both.at[t], SS + n, SCALE + n, partner)

    phase("residual")
    local(res_hbm, res_v, LRES).wait()
    mine = jnp.where(lax.div(f, 2) == t, 1, 0)
    first = mine * x + (1 - mine) * c
    other = mine * f + (1 - mine) * y
    target = own_res.at[f]
    first_lanes = lanes((first - 2 * t) * own_width, own_width)
    other_lanes = lanes((other - 2 * t) * own_width, own_width)
    my_rows, other_rows = pl.ds(t * rows, rows), pl.ds((1 - t) * rows, rows)
    for core in range(2):
        send(
            res_v.at[pl.ds(core * rows, rows), first_lanes], target, SR + core, RES,
            (r, first, core),
        )
    send(res_v.at[other_rows, other_lanes], target, SR + 2, RES, (r, other, 1 - t))
    send(res_v.at[my_rows, other_lanes], target, SR + 3, RES, (r, other, t), when=mine == 0)
    kept_res = pltpu.make_async_copy(res_v.at[my_rows, other_lanes], target, recv_sem.at[RES])
    pl.when(mine == 1)(kept_res.start)

    local(gate_hbm.at[extra_rows], extra_stage, LEXTRA).wait()
    cut_blocks(extra_stage, extra_blocks, 0, extra, second)
    for rel in (1, 2, 3):
        send(
            extra_blocks.at[fs_of[rel]], weight_rows(second, f, kept, extra, t), SX, XN,
            (r, fs_of[rel], t),
        )

    def head_lanes(core, h):
        return lanes((core * heads + h) * head_width, head_width)

    def z_moves():
        for step in range(1, 4):
            to = lax.rem(r + step, 4)
            near = (to - r == 1) | (r - to == 1)
            goes = (r == 1) | (r == 2) | near
            short = (r == 2) | ((r == 1) & (to == 2))
            yield step - 1, to, goes, short

    def pump(n, rel):
        block = weight_at(m, fs_of[rel], n)
        arrive(block, A + n * 3 + rel - 1)
        send(block, block, SD, DN, partner)
        for index, to, goes, short in z_moves():
            slot = ZN + n * 3 + rel - 1
            slot = slot + 6 * jnp.where(short, 1, 0)
            if n == 0:
                send(block, block, SZ + index, slot, (to, f, t), when=goes)
            else:
                send(
                    block, block, SZ + index, slot, (to, f, t),
                    when=goes & jnp.logical_not(short),
                )
                cut = weight_at(m, fs_of[rel], n, kept - early)
                send(cut, cut, SZ + index, slot, (to, f, t), when=goes & short)

    def pump_z(n, rel):
        for which in range(2):
            size = kept - early if n == 1 and which == 1 else None
            block = weight_at(along[which], fs_of[rel], n, size)
            arrive(block, ZN + which * 6 + n * 3 + rel - 1)
            send(block, block, SD, DN, partner)

    surge = jnp.transpose(sg_ref[...])
    for h in range(heads):
        phase("head")
        keys = slice(h * head_width, (h + 1) * head_width)
        local(lo_hbm.at[:, keys], lo_v.at[:, keys], LHEAD + 2 * h).wait()
        wide_keys = slice(0, 3 * head_width)
        local(q_hbm.at[:, wide_keys], q_v.at[:, wide_keys], LHEAD + 2 * h + 1).wait()
        normed[h] = attend_head(
            q_v[:, keys], k_v[:, keys], v_v[:, keys], lo_v[:, keys],
            surge[:, h : h + 1], head_gain_ref[...],
        )
        target = gathered.at[f, :, head_lanes(t, h)]
        for core in range(2):
            for n, to in enumerate((x, y)):
                send(
                    normed.at[h, pl.ds(core * rows, rows)], target, SH + n,
                    CP + t * 4 + h if n == core else CQ, (r, to, core),
                )
        send(normed.at[h, other_rows], target, SH + 2, CO, partner)
        local(normed.at[h, my_rows], target, LKEPT + 1).start()
        if h == heads - 2:
            phase("pump_a0")
            for rel in (1, 2):
                pump(0, rel)
    phase("pump_a0")
    pump(0, 3)

    phase("wo_own_cast")
    local(wo_hbm, wo_f32, LWO).wait()
    wo_half[...] = wo_f32[...].astype(half)
    target = wo_all.at[:, lanes(t * local_width, local_width)]
    send(wo_half, target, SWO, WO, partner)
    local(wo_half, target, LKEPT + 2).start()
    own_lane = lax.broadcasted_iota(jnp.int32, (own_width, units), 1)
    for n in range(2):
        local(gate_hbm.at[:, own_lanes], own_f32.at[n], LOWN + n).wait()
        cut = jnp.where((own_lane < own_spill) & (others[n] == 2), 0.0, own_f32[n])
        own_half[n] = cut.astype(half)
        target = weight_rows(others[n], f, 0, own_width, t)
        send(own_half.at[n], target, SD, DN, partner)
        local(own_half.at[n], target, LKEPT).start()

    phase("pump_a1")
    for rel in (1, 2, 3):
        pump(1, rel)
    arrive(extra_blocks.at[pl.ds(0, 3)], XN)
    for rel in (1, 2, 3):
        block = weight_rows(second, fs_of[rel], kept, extra, t)
        send(block, block, SD, DN, partner)

    phase("relay_c")
    for h in range(heads):
        for core in range(2):
            block = gathered.at[p, :, head_lanes(core, h)]
            arrive(block, CP + core * 4 + h)
            send(block, block, SC, CC, (r, q, t))
    phase("pump_z0")
    for rel in (1, 2, 3):
        pump_z(0, rel)
    pump_z(1, 1)

    phase("wait_small")
    local(own_half, own_half, LKEPT).wait()
    local(own_half.at[0], own_half.at[0], LKEPT).wait()
    target = gathered.at[f, :, lanes(t * local_width, local_width)]
    local(target, target, LKEPT + 1).wait()
    local(wo_half, wo_half, LKEPT + 2).wait()
    for n, both in enumerate((os_all, gs_all, us_all)):
        arrive(both.at[1 - t], SCALE + n)
    arrive(wo_half, WO)
    arrive(own_res, RES)
    out_scale = os_all[lax.div(f, 2), :, lanes(lax.rem(f, 2) * own_width, own_width)]
    order = (f, p, q, c)

    def feature_lanes(owner):
        return lanes(owner * own_width, own_width)

    def share(k, sem, slot, to):
        block = updated.at[order[k], :, feature_lanes(f)]
        send(block, block, sem, slot, (r, to, t))

    for k in range(4):
        seq = order[k]
        phase("wait_c")
        if k == 0:
            arrive(gathered.at[f, :, lanes((1 - t) * local_width, local_width)], CO)
        elif k > 1:
            arrive(gathered.at[seq], (CQ, CC)[k - 2])
        phase("outproj")
        mixed = by_rows(gathered[seq], wo_all[...])
        updated[seq, :, feature_lanes(f)] = (
            own_res[seq].astype(jnp.float32) + out_scale * mixed
        ).astype(half)
        if k == 2:
            for done in (2, 0, 1):
                share(done, SE, EP + (done ^ 1), p)
            for done in (1, 2, 0):
                share(done, SE + 1, EQ + (done ^ 2), q)
        elif k == 3:
            share(k, SE, EP + (k ^ 1), p)
            share(k, SE + 1, EQ + (k ^ 2), q)

    phase("pump_z1")
    pump_z(1, 2)
    phase("relay_e")
    for k in (1, 3, 0, 2):
        block = updated.at[order[k], :, feature_lanes(p)]
        arrive(block, EP + k)
        send(block, block, SE + 2, EC + (k ^ 2), (r, q, t))
    phase("pump_z2")
    pump_z(1, 3)
    phase("wait_w")
    arrive(weights.at[:, :, lanes((1 - t) * units, units)], DN)

    gate_scale = jnp.concatenate([gs_all[0, :, own_lanes], gs_all[1, :, own_lanes]], axis=1)
    up_scale = jnp.concatenate([us_all[0, :, own_lanes], us_all[1, :, own_lanes]], axis=1)

    def piece(n):
        return slice(n * local_width, (n + 1) * local_width)

    for k in (3, 1, 0, 2):
        seq = order[k]
        phase("wait_e")
        arrive(updated.at[seq, :, feature_lanes(q)], EQ + k)
        arrive(updated.at[seq, :, feature_lanes(c)], EC + k)
        phase("gate_up")
        wide = updated[seq].astype(jnp.float32)
        factor = lax.rsqrt(jnp.mean(wide * wide, axis=-1, keepdims=True) + epsilon)
        normin = (wide * factor * mlp_gain_ref[...]).astype(half)
        gate_pre = jnp.dot(normin, weights[0], preferred_element_type=jnp.float32) * gate_scale
        up_pre = jnp.dot(normin, weights[1], preferred_element_type=jnp.float32) * up_scale
        hidden = (jax.nn.silu(gate_pre) * up_pre).astype(half)
        phase("down")
        for n in range(2):
            term = by_rows(hidden, weights[2, piece(n), :])
            if k == 3:
                to_p[n] = term.astype(half)
                send(to_p.at[n], from_p.at[n], SF, FP + n, (r, p, t))
            elif k == 1:
                to_p2[n] = term.astype(half)
                send(to_p2.at[n], from_p2.at[t], SF + 1, FP + 2 + t, (r, p, n))
            elif k == 0:
                own_down[n] = term
            else:
                arrive(from_p.at[n], FP + n)
                to_q[n] = (term + from_p[n].astype(jnp.float32)).astype(half)
                send(to_q.at[n], from_q.at[t], SF + 2, FP + 4 + t, (r, q, n))
        if k == 0:
            send(own_down.at[1 - t], other_down, SO, OUT, partner)
            far_half = updated.at[f, :, lanes((1 - t) * local_width, local_width)]
            send(far_half, other_updated, SO + 1, OUT + 1, partner)

    phase("wait_other")
    arrive(other_down, OUT)
    arrive(other_updated, OUT + 1)
    phase("wait_p2")
    for core in range(2):
        arrive(from_p2.at[core], FP + 2 + core)
    own_sum = own_down[t] + from_p2[t].astype(jnp.float32)
    other_sum = other_down[...] + from_p2[1 - t].astype(jnp.float32)
    phase("wait_q")
    for core in range(2):
        arrive(from_q.at[core], FP + 4 + core)
    for n, (core, total, rows_in) in enumerate((
        (t, own_sum, updated[f, :, lanes(t * local_width, local_width)]),
        (1 - t, other_sum, other_updated[...]),
    )):
        total = total + from_q[core].astype(jnp.float32)
        target = pl.ds(core * rows, rows)
        q_v[target, :] = (rows_in.astype(jnp.float32) + ds_ref[...] * total).astype(half)
        local(q_v.at[target], out_ref.at[target], LEND + n).start()

    phase("drain")
    for rel in (1, 2, 3):
        waiter(blocks.at[0], SA + rel - 1, 0).wait_send()
    waiter(weights.at[:, :, lanes(t * units, units)], SD, 0).wait_send()
    for n, both in enumerate((os_all, gs_all, us_all)):
        waiter(both.at[t], SS + n, 0).wait_send()
    for n in range(3):
        waiter(own_res.at[0], SR + n, 0).wait_send()
    pl.when(mine == 0)(waiter(own_res.at[0], SR + 3, 0).wait_send)
    waiter(extra_blocks.at[pl.ds(0, 3)], SX, 0).wait_send()
    for n in range(2):
        waiter(normed, SH + n, 0).wait_send()
    waiter(normed.at[:, pl.ds(0, rows)], SH + 2, 0).wait_send()
    for index, to, goes, short in z_moves():
        for length, when in (
            (own_width, goes & jnp.logical_not(short)), (kept, goes & short),
        ):
            sent = weights.at[0, pl.ds(0, 3 * length), lanes(0, units)]
            pl.when(when)(waiter(sent, SZ + index, 0).wait_send)
    waiter(wo_half, SWO, 0).wait_send()
    waiter(gathered.at[0], SC, 0).wait_send()
    for n in range(3):
        waiter(updated.at[:, :, pl.ds(0, own_width)], SE + n, 0).wait_send()
    for n, sent in enumerate((to_p, to_p2, to_q)):
        waiter(sent, SF + n, 0).wait_send()
    waiter(other_down, SO, 0).wait_send()
    waiter(other_updated, SO + 1, 0).wait_send()
    for n, core in enumerate((t, 1 - t)):
        target = pl.ds(core * rows, rows)
        local(q_v.at[target], out_ref.at[target], LEND + n).wait()
    phase(None)


def one_kernel_body(
    sizes,
    residual,
    queries,
    key_matrix,
    value_matrix,
    decay_logodds,
    decay_surge,
    head_norm_gain,
    output_matrix,
    output_column_scale,
    premix_norm_gain,
    gate_matrix,
    gate_column_scale,
    up_matrix,
    up_column_scale,
    down_matrix,
    down_column_scale,
):
    half, full = jnp.bfloat16, jnp.float32
    _, tokens, local_width = residual.shape
    rows = tokens // 2
    own_width, total_units = gate_matrix.shape
    width = premix_norm_gain.shape[0]
    heads = decay_surge.shape[2]
    units = -(-total_units // (128 * 4)) * 128
    hbm, vmem = pl.BlockSpec(memory_space=pl.ANY), pl.BlockSpec(memory_space=pltpu.VMEM)
    out = pl.pallas_call(
        layer_kernel,
        out_shape=jax.ShapeDtypeStruct((tokens, local_width), half),
        in_specs=[hbm] * 9 + [vmem] * 7,
        out_specs=hbm,
        scratch_shapes=[
            pltpu.VMEM((tokens, local_width), half),
            pltpu.VMEM((tokens, local_width), half),
            pltpu.VMEM((tokens, local_width), half),
            pltpu.VMEM((tokens, local_width), full),
            pltpu.VMEM((tokens, local_width), half),
            pltpu.VMEM((own_width, local_width), full),
            pltpu.VMEM((own_width, local_width), half),
            pltpu.VMEM((own_width, width), half),
            pltpu.VMEM((own_width, total_units), full),
            pltpu.VMEM((2, own_width, units), full),
            pltpu.VMEM((2, own_width, units), half),
            pltpu.VMEM((4, own_width, units), half),
            pltpu.VMEM((own_width // EXTRA_PART, total_units), full),
            pltpu.VMEM((4, own_width // EXTRA_PART, units), half),
            pltpu.VMEM((3, width, 2 * units), half),
            pltpu.VMEM((heads, tokens, local_width // heads), half),
            pltpu.VMEM((4, rows, width), half),
            pltpu.VMEM((4, rows, own_width), half),
            pltpu.VMEM((4, rows, width), half),
            pltpu.VMEM((2, 1, local_width), full),
            pltpu.VMEM((2, 1, total_units), full),
            pltpu.VMEM((2, 1, total_units), full),
            pltpu.VMEM((2, rows, local_width), full),
            pltpu.VMEM((rows, local_width), full),
            pltpu.VMEM((rows, local_width), half),
        ]
        + [pltpu.VMEM((2, rows, local_width), half)] * 6
        + [
            pltpu.SemaphoreType.DMA((20,)),
            pltpu.SemaphoreType.DMA((28,)),
            pltpu.SemaphoreType.DMA((56,)),
        ],
        compiler_params=pltpu.CompilerParams(
            collective_id=1, has_side_effects=True, vmem_limit_bytes=VMEM_MIB * 2**20
        ),
    )(
        queries[0], key_matrix[0], value_matrix[0], decay_logodds[0], residual[0],
        output_matrix, gate_matrix, up_matrix, down_matrix,
        jnp.transpose(decay_surge[0]), head_norm_gain.reshape(1, -1), premix_norm_gain.reshape(1, -1),
        output_column_scale.reshape(1, -1), gate_column_scale,
        up_column_scale, down_column_scale.reshape(1, -1),
    )
    return out[None]


def greet(devices):
    barrier = pltpu.get_barrier_semaphore()
    for device in devices:
        pl.semaphore_signal(
            barrier, inc=1, device_id=device, device_id_type=pl.DeviceIdType.MESH
        )
    pl.semaphore_wait(barrier, len(devices))


def chosen_body(mesh):
    sizes = tuple(mesh.shape[name] for name in ("rep", "fs", "tp"))

    def run(*args):
        residual, surge, output_matrix, gate_matrix = args[0], args[5], args[7], args[10]
        sequences, tokens, local_width = residual.shape
        own_width, total_units = gate_matrix.shape
        fits = (
            sizes == (4, 4, 2)
            and sequences == 1
            and tokens % (2 * BLOCK) == 0
            and local_width == 2 * own_width
            and output_matrix.shape == (own_width, local_width)
            and own_width % 128 == 0
            and total_units % 128 == 0
            and total_units >= 512
            and (local_width // surge.shape[2]) % 128 == 0
            and surge.shape[2] == 4
        )
        if fits:
            return one_kernel_body(sizes, *args)
        return body(*args)

    return run


def solution(mesh):
    return jax.shard_map(
        chosen_body(mesh),
        mesh=mesh,
        in_specs=(
            P(("rep", "fs"), None, "tp"),
            P(("rep", "fs"), None, "tp"),
            P(("rep", "fs"), None, "tp"),
            P(("rep", "fs"), None, "tp"),
            P(("rep", "fs"), None, "tp"),
            P(("rep", "fs"), None, "tp"),
            P(),
            P("fs", "tp"),
            P("tp"),
            P(),
            P("fs", "tp"),
            P("tp"),
            P("fs", "tp"),
            P("tp"),
            P("fs", "tp"),
            P("tp"),
        ),
        out_specs=P(("rep", "fs"), None, "tp"),
        check_vma=False,
    )
```

time: 125 us -> 86.8 us (0.69)
  Pallas kernels: 118 us -> 84.7 us
  local copies, waits for them, and re-layouts: 5.93 us -> 1.87 us
    pallas_call x1, Pallas kernels: 118 us -> 84.7 us  [one_kernel_body(): pl.pallas_call(layer_kernel, out_shape=jax.ShapeDtypeStruct((tokens, loca...]
    reshape x2 -> x0, local copies, waits for them, and re-layouts: 2.58 us -> none  [the longest x1 1.29 us: one_kernel_body(): gate_column_scale.reshape(1, -1)]
    unnamed x2 -> x1, local copies, waits for them, and re-layouts: 3.35 us -> 1.87 us
where the time goes in v2:
time: 86.8 us; the launch traced here: 86.6 us
  Pallas kernels  84.7 us (98%)
  local copies, waits for them, and re-layouts  1.87 us (2%)
    pallas_call x1, Pallas kernels, one_kernel_body(): pl.pallas_call(layer_kernel, out_shape=jax.ShapeDtypeStruct((tokens, loca...  84.7 us
    unnamed x1, local copies, waits for them, and re-layouts  1.87 us

profile of v2, /device:TPU:1, one launch (start us, length us, event | category | flops | bytes accessed | tf_op | source)
XLA Modules:
  0.0 86.6 jit_solution(8477255937563710489)
XLA Ops:
  0.0 84.7 %shard_map.154 = bf16[256,1024]{1,0:T(8,128)(2,1)} custom-call(bf16[256,1024]{1,0:T(8,128)(2,1)} %bitcast.15, bf16[256,1024]{1,0:T(8,128)(2,1)} %bitcast.16, bf16[256,1024]{1,0:T(8,128)(2,1)} %bitcast.17, f32[256,1024]{1,0:T(8,128)} %bitcast.14, bf16[256,1024]{1,0:T(8,128)(2,1)} %bitcast.18, f32[512,1024]{1,0:T(8,128)} %wo_hbm.1, f32[512,1408]{1,0:T(8,128)} %gate_hbm.1, ...), custom_call_target="tpu_custom_call" | custom-call | tf_op jit(solution)/shard_map/pallas_call | solution.py:636
  84.7 1.9 %copy.18 = bf16[1,256,1024]{2,1,0:T(8,128)(2,1)} copy(bf16[1,256,1024]{2,1,0:T(8,128)(2,1)} %bitcast.13) | data formatting | bytes 1048576

commit v3 on v2

--- a/solution.py
+++ b/solution.py
@@ -180,14 +180,15 @@
 
 
 VMEM_MIB = 60
-EARLY_PART = 4
 EXTRA_PART = 8
+AFTER_HEAD = ((), ((0, 1), (0, 2)), ((0, 3),), ((1, 1), (1, 2)))
 
 
 def layer_kernel(
     q_hbm, k_hbm, v_hbm, lo_hbm, res_hbm, wo_hbm, gate_hbm, up_hbm, down_hbm,
+    sg_hbm, head_gain_hbm, mlp_gain_hbm, os_hbm, gs_hbm, us_hbm, ds_hbm,
+    out_ref,
     sg_ref, head_gain_ref, mlp_gain_ref, os_ref, gs_ref, us_ref, ds_ref,
-    out_ref,
     q_v, k_v, v_v, lo_v, res_v, wo_f32, wo_half, wo_all,
     stage, own_f32, own_half, blocks, extra_stage, extra_blocks, weights,
     normed, gathered, own_res, updated, os_all, gs_all, us_all,
@@ -213,14 +214,18 @@
     heads = sg_ref.shape[0]
     head_width = local_width // heads
     starts = [min(j * units, total_units - units) for j in range(4)]
-    early, extra = own_width // EARLY_PART, own_width // EXTRA_PART
-    pieces = ((0, early), (early, own_width - early))
+    eighth, extra = own_width // 8, own_width // EXTRA_PART
+    pieces = (
+        (0, eighth), (eighth, 3 * eighth), (4 * eighth, 4 * eighth - extra),
+        (own_width - extra, extra),
+    )
+    last = len(pieces) - 1
     kept = own_width - extra
 
     SA, SD, SS, SR, SX, SH, SZ, SWO, SC, SE, SF, SO = 0, 3, 4, 7, 11, 12, 15, 18, 19, 20, 23, 26
-    A, RES, CP, CQ, CC, CO, WO, SCALE = 0, 6, 7, 15, 16, 17, 18, 19
-    EP, EQ, EC, ZN, DN, XN, FP, OUT = 22, 26, 30, 34, 46, 47, 48, 54
-    LSTAGE, LEXTRA, LRES, LHEAD, LWO, LOWN, LKEPT, LEND = 0, 2, 3, 4, 12, 13, 15, 18
+    A, RES, CP, CQ, CC, CO, WO, SCALE = 0, 12, 13, 21, 22, 23, 24, 25
+    EP, EQ, EC, ZN, DN, XN, FP, OUT = 28, 32, 36, 40, 64, 66, 67, 73
+    LSTAGE, LEXTRA, LRES, LHEAD, LWO, LOWN, LKEPT, LEND, LSMALL = 0, 4, 5, 6, 14, 15, 17, 20, 22
 
     def lanes(start, size):
         return pl.ds(pl.multiple_of(start, 128), size)
@@ -273,11 +278,17 @@
     own_spill = f * units - own_start
     own_lanes = lanes(own_start, units)
     extra_rows = pl.ds(kept, extra)
-    for n in range(2):
+    for n in range(len(pieces)):
         for mm in range(3):
             @pl.when(m == mm)
             def _(mm=mm, n=n):
                 local(mats[mm].at[part(n)], stage.at[part(n)], LSTAGE + n).start()
+    small = (
+        (os_hbm, os_ref), (gs_hbm, gs_ref), (us_hbm, us_ref), (sg_hbm, sg_ref),
+        (head_gain_hbm, head_gain_ref), (mlp_gain_hbm, mlp_gain_ref), (ds_hbm, ds_ref),
+    )
+    for n, (source, target) in enumerate(small):
+        local(source, target, LSMALL + n).start()
     local(res_hbm, res_v, LRES).start()
     for mm in (1, 2):
         @pl.when(second == mm)
@@ -301,16 +312,22 @@
     peers = [partner]
     for other in (x, y, c):
         peers += [(r, other, 0), (r, other, 1)]
-    peers += [(lax.rem(r + step, 4), f, t) for step in range(1, 4)]
-    greet(peers)
+    middle = (r == 1) | (r == 2)
+    beside = jnp.where(r < 2, r + 1, r - 1)
+    away = jnp.where(r < 2, r + 2, r - 2)
+    peers += [(beside, f, t), (away, f, t)]
+    greet(peers, middle, (jnp.where(r < 2, 0, 3), f, t))
 
     def weight_rows(matrix, owner, start, size, core):
         return weights.at[
             matrix, pl.ds(owner * own_width + start, size), lanes(core * units, units)
         ]
 
-    def weight_at(matrix, owner, n, size=None):
-        return weight_rows(matrix, owner, pieces[n][0], size or pieces[n][1], t)
+    def weight_at(matrix, owner, n):
+        return weight_rows(matrix, owner, *pieces[n], t)
+
+    def dn(matrix):
+        return DN + jnp.where(matrix == 2, 1, 0)
 
     def cut_blocks(source, target, start, size, matrix):
         lane = lax.broadcasted_iota(jnp.int32, (size, units), 1)
@@ -323,7 +340,7 @@
             target[j, span, :] = cut.astype(half)
 
     phase("cut_send")
-    for n in range(2):
+    for n in range(len(pieces)):
         local(gate_hbm.at[part(n)], stage.at[part(n)], LSTAGE + n).wait()
         cut_blocks(stage, blocks, *pieces[n], m)
         for rel in (1, 2, 3):
@@ -333,8 +350,10 @@
             )
     target = weight_rows(m, f, 0, own_width, t)
     local(blocks.at[f], target, LKEPT).start()
-    send(blocks.at[f], target, SD, DN, partner)
-
+    send(blocks.at[f], target, SD, dn(m), partner)
+
+    for n, (source, target) in enumerate(small):
+        local(source, target, LSMALL + n).wait()
     for n, (ref, both) in enumerate(((os_ref, os_all), (gs_ref, gs_all), (us_ref, us_all))):
         both[t] = ref[...].reshape(1, -1)
         send(both.at[t], both.at[t], SS + n, SCALE + n, partner)
@@ -360,7 +379,7 @@
 
     local(gate_hbm.at[extra_rows], extra_stage, LEXTRA).wait()
     cut_blocks(extra_stage, extra_blocks, 0, extra, second)
-    for rel in (1, 2, 3):
+    for rel in (1, 2):
         send(
             extra_blocks.at[fs_of[rel]], weight_rows(second, f, kept, extra, t), SX, XN,
             (r, fs_of[rel], t),
@@ -380,26 +399,21 @@
     def pump(n, rel):
         block = weight_at(m, fs_of[rel], n)
         arrive(block, A + n * 3 + rel - 1)
-        send(block, block, SD, DN, partner)
+        send(block, block, SD, dn(m), partner)
         for index, to, goes, short in z_moves():
             slot = ZN + n * 3 + rel - 1
-            slot = slot + 6 * jnp.where(short, 1, 0)
-            if n == 0:
-                send(block, block, SZ + index, slot, (to, f, t), when=goes)
-            else:
-                send(
-                    block, block, SZ + index, slot, (to, f, t),
-                    when=goes & jnp.logical_not(short),
-                )
-                cut = weight_at(m, fs_of[rel], n, kept - early)
-                send(cut, cut, SZ + index, slot, (to, f, t), when=goes & short)
+            slot = slot + 12 * jnp.where(short, 1, 0)
+            if n == last and rel < 3:
+                goes = goes & jnp.logical_not(short)
+            send(block, block, SZ + index, slot, (to, f, t), when=goes)
 
     def pump_z(n, rel):
         for which in range(2):
-            size = kept - early if n == 1 and which == 1 else None
-            block = weight_at(along[which], fs_of[rel], n, size)
-            arrive(block, ZN + which * 6 + n * 3 + rel - 1)
-            send(block, block, SD, DN, partner)
+            if which == 1 and n == last and rel < 3:
+                continue
+            block = weight_at(along[which], fs_of[rel], n)
+            arrive(block, ZN + which * 12 + n * 3 + rel - 1)
+            send(block, block, SD, dn(along[which]), partner)
 
     surge = jnp.transpose(sg_ref[...])
     for h in range(heads):
@@ -421,17 +435,14 @@
                 )
         send(normed.at[h, other_rows], target, SH + 2, CO, partner)
         local(normed.at[h, my_rows], target, LKEPT + 1).start()
-        if h == heads - 2:
-            phase("pump_a0")
-            for rel in (1, 2):
-                pump(0, rel)
-    phase("pump_a0")
-    pump(0, 3)
+        phase(f"pump_a#h={h}")
+        for n, rel in AFTER_HEAD[h]:
+            pump(n, rel)
 
     phase("wo_own_cast")
     local(wo_hbm, wo_f32, LWO).wait()
-    wo_half[...] = wo_f32[...].astype(half)
-    target = wo_all.at[:, lanes(t * local_width, local_width)]
+    wo_half[...] = jnp.transpose(wo_f32[...].astype(half))
+    target = wo_all.at[pl.ds(t * local_width, local_width)]
     send(wo_half, target, SWO, WO, partner)
     local(wo_half, target, LKEPT + 2).start()
     own_lane = lax.broadcasted_iota(jnp.int32, (own_width, units), 1)
@@ -440,16 +451,16 @@
         cut = jnp.where((own_lane < own_spill) & (others[n] == 2), 0.0, own_f32[n])
         own_half[n] = cut.astype(half)
         target = weight_rows(others[n], f, 0, own_width, t)
-        send(own_half.at[n], target, SD, DN, partner)
+        send(own_half.at[n], target, SD, dn(others[n]), partner)
         local(own_half.at[n], target, LKEPT).start()
 
     phase("pump_a1")
-    for rel in (1, 2, 3):
-        pump(1, rel)
-    arrive(extra_blocks.at[pl.ds(0, 3)], XN)
-    for rel in (1, 2, 3):
+    for n, rel in ((1, 3), (2, 1), (2, 2), (2, 3), (3, 1), (3, 2), (3, 3)):
+        pump(n, rel)
+    arrive(extra_blocks.at[pl.ds(0, 2)], XN)
+    for rel in (1, 2):
         block = weight_rows(second, fs_of[rel], kept, extra, t)
-        send(block, block, SD, DN, partner)
+        send(block, block, SD, dn(second), partner)
 
     phase("relay_c")
     for h in range(heads):
@@ -458,9 +469,9 @@
             arrive(block, CP + core * 4 + h)
             send(block, block, SC, CC, (r, q, t))
     phase("pump_z0")
-    for rel in (1, 2, 3):
-        pump_z(0, rel)
-    pump_z(1, 1)
+    for n in (0, 1):
+        for rel in (1, 2, 3):
+            pump_z(n, rel)
 
     phase("wait_small")
     local(own_half, own_half, LKEPT).wait()
@@ -482,6 +493,11 @@
         block = updated.at[order[k], :, feature_lanes(f)]
         send(block, block, sem, slot, (r, to, t))
 
+    def relay(k):
+        block = updated.at[order[k], :, feature_lanes(p)]
+        arrive(block, EP + k)
+        send(block, block, SE + 2, EC + (k ^ 2), (r, q, t))
+
     for k in range(4):
         seq = order[k]
         phase("wait_c")
@@ -490,30 +506,35 @@
         elif k > 1:
             arrive(gathered.at[seq], (CQ, CC)[k - 2])
         phase("outproj")
-        mixed = by_rows(gathered[seq], wo_all[...])
+        mixed = jnp.dot(gathered[seq], wo_all[...], preferred_element_type=jnp.float32)
         updated[seq, :, feature_lanes(f)] = (
             own_res[seq].astype(jnp.float32) + out_scale * mixed
         ).astype(half)
         if k == 2:
             for done in (2, 0, 1):
                 share(done, SE, EP + (done ^ 1), p)
-            for done in (1, 2, 0):
+            for done in (1, 2):
                 share(done, SE + 1, EQ + (done ^ 2), q)
         elif k == 3:
-            share(k, SE, EP + (k ^ 1), p)
-            share(k, SE + 1, EQ + (k ^ 2), q)
+            share(3, SE, EP + 2, p)
+            relay(1)
+            for done in (3, 0):
+                share(done, SE + 1, EQ + (done ^ 2), q)
 
     phase("pump_z1")
-    pump_z(1, 2)
+    pump_z(2, 1)
     phase("relay_e")
-    for k in (1, 3, 0, 2):
-        block = updated.at[order[k], :, feature_lanes(p)]
-        arrive(block, EP + k)
-        send(block, block, SE + 2, EC + (k ^ 2), (r, q, t))
+    relay(3)
+    relay(0)
+    phase("pump_z15")
+    pump_z(2, 2)
+    phase("relay_e")
+    relay(2)
     phase("pump_z2")
-    pump_z(1, 3)
+    for n, rel in ((2, 3), (3, 1), (3, 2), (3, 3)):
+        pump_z(n, rel)
     phase("wait_w")
-    arrive(weights.at[:, :, lanes((1 - t) * units, units)], DN)
+    arrive(weights.at[pl.ds(0, 2), :, lanes((1 - t) * units, units)], DN)
 
     gate_scale = jnp.concatenate([gs_all[0, :, own_lanes], gs_all[1, :, own_lanes]], axis=1)
     up_scale = jnp.concatenate([us_all[0, :, own_lanes], us_all[1, :, own_lanes]], axis=1)
@@ -534,6 +555,8 @@
         up_pre = jnp.dot(normin, weights[1], preferred_element_type=jnp.float32) * up_scale
         hidden = (jax.nn.silu(gate_pre) * up_pre).astype(half)
         phase("down")
+        if k == 3:
+            arrive(weights.at[2, :, lanes((1 - t) * units, units)], DN + 1)
         for n in range(2):
             term = by_rows(hidden, weights[2, piece(n), :])
             if k == 3:
@@ -582,15 +605,16 @@
     for n in range(3):
         waiter(own_res.at[0], SR + n, 0).wait_send()
     pl.when(mine == 0)(waiter(own_res.at[0], SR + 3, 0).wait_send)
-    waiter(extra_blocks.at[pl.ds(0, 3)], SX, 0).wait_send()
+    waiter(extra_blocks.at[pl.ds(0, 2)], SX, 0).wait_send()
     for n in range(2):
         waiter(normed, SH + n, 0).wait_send()
     waiter(normed.at[:, pl.ds(0, rows)], SH + 2, 0).wait_send()
     for index, to, goes, short in z_moves():
         for length, when in (
-            (own_width, goes & jnp.logical_not(short)), (kept, goes & short),
+            (3 * own_width, goes & jnp.logical_not(short)),
+            (3 * own_width - 2 * extra, goes & short),
         ):
-            sent = weights.at[0, pl.ds(0, 3 * length), lanes(0, units)]
+            sent = weights.at[0, pl.ds(0, length), lanes(0, units)]
             pl.when(when)(waiter(sent, SZ + index, 0).wait_send)
     waiter(wo_half, SWO, 0).wait_send()
     waiter(gathered.at[0], SC, 0).wait_send()
@@ -632,21 +656,28 @@
     width = premix_norm_gain.shape[0]
     heads = decay_surge.shape[2]
     units = -(-total_units // (128 * 4)) * 128
-    hbm, vmem = pl.BlockSpec(memory_space=pl.ANY), pl.BlockSpec(memory_space=pltpu.VMEM)
+    hbm = pl.BlockSpec(memory_space=pl.ANY)
     out = pl.pallas_call(
         layer_kernel,
         out_shape=jax.ShapeDtypeStruct((tokens, local_width), half),
-        in_specs=[hbm] * 9 + [vmem] * 7,
+        in_specs=[hbm] * 16,
         out_specs=hbm,
         scratch_shapes=[
+            pltpu.VMEM((heads, tokens), full),
+            pltpu.VMEM((1, head_norm_gain.shape[0]), full),
+            pltpu.VMEM((1, width), full),
+            pltpu.VMEM((1, local_width), full),
+            pltpu.VMEM((total_units,), full),
+            pltpu.VMEM((total_units,), full),
+            pltpu.VMEM((1, local_width), full),
             pltpu.VMEM((tokens, local_width), half),
             pltpu.VMEM((tokens, local_width), half),
             pltpu.VMEM((tokens, local_width), half),
             pltpu.VMEM((tokens, local_width), full),
             pltpu.VMEM((tokens, local_width), half),
             pltpu.VMEM((own_width, local_width), full),
-            pltpu.VMEM((own_width, local_width), half),
-            pltpu.VMEM((own_width, width), half),
+            pltpu.VMEM((local_width, own_width), half),
+            pltpu.VMEM((width, own_width), half),
             pltpu.VMEM((own_width, total_units), full),
             pltpu.VMEM((2, own_width, units), full),
             pltpu.VMEM((2, own_width, units), half),
@@ -667,9 +698,9 @@
         ]
         + [pltpu.VMEM((2, rows, local_width), half)] * 6
         + [
-            pltpu.SemaphoreType.DMA((20,)),
+            pltpu.SemaphoreType.DMA((29,)),
             pltpu.SemaphoreType.DMA((28,)),
-            pltpu.SemaphoreType.DMA((56,)),
+            pltpu.SemaphoreType.DMA((75,)),
         ],
         compiler_params=pltpu.CompilerParams(
             collective_id=1, has_side_effects=True, vmem_limit_bytes=VMEM_MIB * 2**20
@@ -684,13 +715,18 @@
     return out[None]
 
 
-def greet(devices):
+def greet(devices, more, extra):
     barrier = pltpu.get_barrier_semaphore()
-    for device in devices:
+
+    def signal(device):
         pl.semaphore_signal(
             barrier, inc=1, device_id=device, device_id_type=pl.DeviceIdType.MESH
         )
-    pl.semaphore_wait(barrier, len(devices))
+
+    for device in devices:
+        signal(device)
+    pl.when(more)(lambda: signal(extra))
+    pl.semaphore_wait(barrier, len(devices) + jnp.where(more, 1, 0))
 
 
 def chosen_body(mesh):

time: 86.8 us -> 84 us (0.968)
  Pallas kernels: 84.7 us -> 82 us
    pallas_call x1, Pallas kernels: 84.7 us -> 82 us  [one_kernel_body(): pl.pallas_call(layer_kernel, out_shape=jax.ShapeDtypeStruct((tokens, loca...]
where the time goes in v3:
time: 84 us; the launch traced here: 83.9 us
  Pallas kernels  82 us (98%)
  local copies, waits for them, and re-layouts  1.87 us (2%)
    pallas_call x1, Pallas kernels, one_kernel_body(): pl.pallas_call(layer_kernel, out_shape=jax.ShapeDtypeStruct((tokens, loca...  82 us
    unnamed x1, local copies, waits for them, and re-layouts  1.87 us

profile of v3, /device:TPU:1, one launch (start us, length us, event | category | flops | bytes accessed | tf_op | source)
XLA Modules:
  0.0 83.9 jit_solution(4406182943151443622)
XLA Ops:
  0.0 82.0 %shard_map.154 = bf16[256,1024]{1,0:T(8,128)(2,1)} custom-call(bf16[256,1024]{1,0:T(8,128)(2,1)} %bitcast.15, bf16[256,1024]{1,0:T(8,128)(2,1)} %bitcast.16, bf16[256,1024]{1,0:T(8,128)(2,1)} %bitcast.17, f32[256,1024]{1,0:T(8,128)} %bitcast.14, bf16[256,1024]{1,0:T(8,128)(2,1)} %bitcast.18, f32[512,1024]{1,0:T(8,128)} %wo_hbm.1, f32[512,1408]{1,0:T(8,128)} %gate_hbm.1, ...), custom_call_target="tpu_custom_call" | custom-call | tf_op jit(solution)/shard_map/pallas_call | solution.py:660
  82.0 1.9 %copy.18 = bf16[1,256,1024]{2,1,0:T(8,128)(2,1)} copy(bf16[1,256,1024]{2,1,0:T(8,128)(2,1)} %bitcast.13) | data formatting | bytes 1048576

commit v4 on v3

--- a/solution.py
+++ b/solution.py
@@ -180,7 +180,7 @@
 
 
 VMEM_MIB = 60
-EXTRA_PART = 8
+EXTRA = (1,)
 AFTER_HEAD = ((), ((0, 1), (0, 2)), ((0, 3),), ((1, 1), (1, 2)))
 
 
@@ -201,37 +201,33 @@
     p, q = x + t * (y - x), y + t * (x - y)
     fs_of = (f, x, y, c)
     partner = (r, f, 1 - t)
-    m = lax.rem(r, 3)
-    zero, second = jnp.where(m == 0, 1, 0), jnp.where(m == 2, 1, 2)
-    along = (zero, second)
-    others = (lax.rem(m + 1, 3), lax.rem(m + 2, 3))
+    z_one = r + 1 - 2 * lax.rem(r, 2)
+    z_two = jnp.where(r < 2, 2, 1)
+    z_three = 6 - r - z_one - z_two
+    middle = (r == 1) | (r == 2)
+    end = jnp.logical_not(middle)
+    pair = lax.div(f, 2)
+    soon, next_, late = (
+        (x + pair * (y - x), 1 + pair), (y + pair * (c - y), 2 + pair),
+        (c + pair * (x - c), 3 - 2 * pair),
+    )
     mats = (gate_hbm, up_hbm, down_hbm)
     tokens, local_width = res_v.shape
     rows = tokens // 2
-    own_width, total_units = stage.shape
-    units = blocks.shape[2]
+    own_width, total_units = wo_f32.shape[0], stage.shape[2]
+    units = blocks.shape[3]
+    quarter = stage.shape[1]
     width = updated.shape[2]
     heads = sg_ref.shape[0]
     head_width = local_width // heads
     starts = [min(j * units, total_units - units) for j in range(4)]
-    eighth, extra = own_width // 8, own_width // EXTRA_PART
-    pieces = (
-        (0, eighth), (eighth, 3 * eighth), (4 * eighth, 4 * eighth - extra),
-        (own_width - extra, extra),
-    )
-    last = len(pieces) - 1
-    kept = own_width - extra
-
-    SA, SD, SS, SR, SX, SH, SZ, SWO, SC, SE, SF, SO = 0, 3, 4, 7, 11, 12, 15, 18, 19, 20, 23, 26
-    A, RES, CP, CQ, CC, CO, WO, SCALE = 0, 12, 13, 21, 22, 23, 24, 25
-    EP, EQ, EC, ZN, DN, XN, FP, OUT = 28, 32, 36, 40, 64, 66, 67, 73
-    LSTAGE, LEXTRA, LRES, LHEAD, LWO, LOWN, LKEPT, LEND, LSMALL = 0, 4, 5, 6, 14, 15, 17, 20, 22
+    SA, SD, SS, SR, SH, SZ, SWO, SC, SE, SF, SO, SX = 0, 3, 4, 7, 11, 14, 17, 18, 19, 22, 25, 27
+    A, RES, CP, CQ, CC, CO, WO, SCALE = 0, 9, 10, 18, 19, 20, 21, 22
+    EP, EQ, EC, ZN, DN, FP, OUT = 25, 29, 33, 37, 73, 76, 82
+    LSTAGE, LRES, LHEAD, LWO, LOWN, LKEPT, LEND, LSMALL, LEXTRA = 0, 3, 4, 12, 13, 16, 19, 21, 28
 
     def lanes(start, size):
         return pl.ds(pl.multiple_of(start, 128), size)
-
-    def part(n):
-        return pl.ds(*pieces[n])
 
     def local(source, target, sem):
         return pltpu.make_async_copy(source, target, load_sem.at[sem])
@@ -277,12 +273,9 @@
     own_start = jnp.minimum(f * units, total_units - units)
     own_spill = f * units - own_start
     own_lanes = lanes(own_start, units)
-    extra_rows = pl.ds(kept, extra)
-    for n in range(len(pieces)):
-        for mm in range(3):
-            @pl.when(m == mm)
-            def _(mm=mm, n=n):
-                local(mats[mm].at[part(n)], stage.at[part(n)], LSTAGE + n).start()
+    my_quarter = pl.ds(pl.multiple_of(r * quarter, quarter), quarter)
+    for mm in range(3):
+        local(mats[mm].at[my_quarter], stage.at[mm], LSTAGE + mm).start()
     small = (
         (os_hbm, os_ref), (gs_hbm, gs_ref), (us_hbm, us_ref), (sg_hbm, sg_ref),
         (head_gain_hbm, head_gain_ref), (mlp_gain_hbm, mlp_gain_ref), (ds_hbm, ds_ref),
@@ -290,29 +283,26 @@
     for n, (source, target) in enumerate(small):
         local(source, target, LSMALL + n).start()
     local(res_hbm, res_v, LRES).start()
-    for mm in (1, 2):
-        @pl.when(second == mm)
-        def _(mm=mm):
-            local(mats[mm].at[extra_rows], extra_stage, LEXTRA).start()
     for h in range(heads):
         keys = slice(h * head_width, (h + 1) * head_width)
         local(lo_hbm.at[:, keys], lo_v.at[:, keys], LHEAD + 2 * h).start()
         for a, b in ((q_hbm, q_v), (k_hbm, k_v), (v_hbm, v_v)):
             local(a.at[:, keys], b.at[:, keys], LHEAD + 2 * h + 1).start()
     local(wo_hbm, wo_f32, LWO).start()
-    for n in range(2):
-        for mm in range(3):
-            @pl.when(m == mm)
-            def _(mm=mm, n=n):
-                local(
-                    mats[(mm + 1 + n) % 3].at[:, own_lanes], own_f32.at[n], LOWN + n
-                ).start()
+    for mm in range(3):
+        local(mats[mm].at[:, own_lanes], own_f32.at[mm], LOWN + mm).start()
+    far_quarter = pl.ds(pl.multiple_of(z_three * quarter, quarter), quarter)
+    extra_loads = [
+        local(mats[mm].at[far_quarter], extra_stage.at[n], LEXTRA + n)
+        for n, mm in enumerate(EXTRA)
+    ]
+    for copy in extra_loads:
+        pl.when(end)(copy.start)
 
     phase("greet")
     peers = [partner]
     for other in (x, y, c):
         peers += [(r, other, 0), (r, other, 1)]
-    middle = (r == 1) | (r == 2)
     beside = jnp.where(r < 2, r + 1, r - 1)
     away = jnp.where(r < 2, r + 2, r - 2)
     peers += [(beside, f, t), (away, f, t)]
@@ -323,34 +313,27 @@
             matrix, pl.ds(owner * own_width + start, size), lanes(core * units, units)
         ]
 
-    def weight_at(matrix, owner, n):
-        return weight_rows(matrix, owner, *pieces[n], t)
-
-    def dn(matrix):
-        return DN + jnp.where(matrix == 2, 1, 0)
-
-    def cut_blocks(source, target, start, size, matrix):
-        lane = lax.broadcasted_iota(jnp.int32, (size, units), 1)
-        span = slice(start, start + size)
+    def dn(matrix, owner):
+        return DN if matrix < 2 else DN + 1 + lax.div(owner, 2)
+
+    def cut_blocks(mm, source, target):
+        lane = lax.broadcasted_iota(jnp.int32, (quarter, units), 1)
         for j in range(4):
-            cut = source[span, starts[j] : starts[j] + units]
+            cut = source[:, starts[j] : starts[j] + units]
             spill = j * units - starts[j]
-            if spill > 0:
-                cut = jnp.where((lane < spill) & (matrix == 2), 0.0, cut)
-            target[j, span, :] = cut.astype(half)
+            if spill > 0 and mm == 2:
+                cut = jnp.where(lane < spill, 0.0, cut)
+            target[j] = cut.astype(half)
 
     phase("cut_send")
-    for n in range(len(pieces)):
-        local(gate_hbm.at[part(n)], stage.at[part(n)], LSTAGE + n).wait()
-        cut_blocks(stage, blocks, *pieces[n], m)
+    for mm in range(3):
+        local(mats[mm].at[my_quarter], stage.at[mm], LSTAGE + mm).wait()
+        cut_blocks(mm, stage.at[mm], blocks.at[mm])
         for rel in (1, 2, 3):
             send(
-                blocks.at[fs_of[rel], part(n)], weight_at(m, f, n),
-                SA + rel - 1, A + n * 3 + rel - 1, (r, fs_of[rel], t),
+                blocks.at[mm, fs_of[rel]], weight_rows(mm, f, r * quarter, quarter, t),
+                SA + rel - 1, A + mm * 3 + rel - 1, (r, fs_of[rel], t),
             )
-    target = weight_rows(m, f, 0, own_width, t)
-    local(blocks.at[f], target, LKEPT).start()
-    send(blocks.at[f], target, SD, dn(m), partner)
 
     for n, (source, target) in enumerate(small):
         local(source, target, LSMALL + n).wait()
@@ -377,43 +360,41 @@
     kept_res = pltpu.make_async_copy(res_v.at[my_rows, other_lanes], target, recv_sem.at[RES])
     pl.when(mine == 1)(kept_res.start)
 
-    local(gate_hbm.at[extra_rows], extra_stage, LEXTRA).wait()
-    cut_blocks(extra_stage, extra_blocks, 0, extra, second)
-    for rel in (1, 2):
-        send(
-            extra_blocks.at[fs_of[rel]], weight_rows(second, f, kept, extra, t), SX, XN,
-            (r, fs_of[rel], t),
-        )
-
     def head_lanes(core, h):
         return lanes((core * heads + h) * head_width, head_width)
 
-    def z_moves():
-        for step in range(1, 4):
-            to = lax.rem(r + step, 4)
-            near = (to - r == 1) | (r - to == 1)
-            goes = (r == 1) | (r == 2) | near
-            short = (r == 2) | ((r == 1) & (to == 2))
-            yield step - 1, to, goes, short
-
-    def pump(n, rel):
-        block = weight_at(m, fs_of[rel], n)
-        arrive(block, A + n * 3 + rel - 1)
-        send(block, block, SD, dn(m), partner)
-        for index, to, goes, short in z_moves():
-            slot = ZN + n * 3 + rel - 1
-            slot = slot + 12 * jnp.where(short, 1, 0)
-            if n == last and rel < 3:
-                goes = goes & jnp.logical_not(short)
-            send(block, block, SZ + index, slot, (to, f, t), when=goes)
-
-    def pump_z(n, rel):
-        for which in range(2):
-            if which == 1 and n == last and rel < 3:
-                continue
-            block = weight_at(along[which], fs_of[rel], n)
-            arrive(block, ZN + which * 12 + n * 3 + rel - 1)
-            send(block, block, SD, dn(along[which]), partner)
+    def piece_of(matrix, owner, plane):
+        return weight_rows(matrix, owner, plane * quarter, quarter, t)
+
+    def z_slot(matrix, rel, plane):
+        return ZN + plane * 9 + matrix * 3 + rel - 1
+
+    def pump(matrix, rel):
+        block, slot = piece_of(matrix, fs_of[rel], r), z_slot(matrix, rel, r)
+        arrive(block, A + matrix * 3 + rel - 1)
+        when = end | (late[1] != rel) if matrix == 2 else None
+        send(block, block, SZ, slot, (z_one, f, t), when)
+        send(block, block, SZ + 1, slot, (z_two, f, t))
+        send(block, block, SD, dn(matrix, fs_of[rel]), partner)
+
+    def pump_late():
+        owner, rel = late
+        block = piece_of(2, owner, r)
+        send(block, block, SZ, z_slot(2, rel, r), (z_one, f, t), middle)
+
+    def pump_z(which, when, todo):
+        for matrix, (owner, rel) in todo:
+            for source in which:
+                plane = (z_one, z_two, z_three)[source]
+                block, slot = piece_of(matrix, owner, plane), z_slot(matrix, rel, plane)
+                pl.when(when)(waiter(block, 0, slot).wait_recv)
+                direct = source == 2 and matrix in EXTRA and rel < 3
+                if when is middle and source > 0 and not direct:
+                    send(block, block, SZ + 2, slot, (z_one, f, t), when)
+                send(block, block, SD, dn(matrix, owner), partner, when)
+
+    gates = [(0, (fs_of[rel], rel)) for rel in (1, 2, 3)]
+    ups = [(1, (fs_of[rel], rel)) for rel in (1, 2, 3)]
 
     surge = jnp.transpose(sg_ref[...])
     for h in range(heads):
@@ -446,21 +427,33 @@
     send(wo_half, target, SWO, WO, partner)
     local(wo_half, target, LKEPT + 2).start()
     own_lane = lax.broadcasted_iota(jnp.int32, (own_width, units), 1)
-    for n in range(2):
-        local(gate_hbm.at[:, own_lanes], own_f32.at[n], LOWN + n).wait()
-        cut = jnp.where((own_lane < own_spill) & (others[n] == 2), 0.0, own_f32[n])
-        own_half[n] = cut.astype(half)
-        target = weight_rows(others[n], f, 0, own_width, t)
-        send(own_half.at[n], target, SD, dn(others[n]), partner)
-        local(own_half.at[n], target, LKEPT).start()
+    for mm in range(3):
+        local(mats[mm].at[:, own_lanes], own_f32.at[mm], LOWN + mm).wait()
+        cut = own_f32[mm]
+        if mm == 2:
+            cut = jnp.where(own_lane < own_spill, 0.0, cut)
+        own_half[mm] = cut.astype(half)
+        target = weight_rows(mm, f, 0, own_width, t)
+        send(own_half.at[mm], target, SD, dn(mm, f), partner)
+        local(own_half.at[mm], target, LKEPT).start()
+
+    phase("extras")
+    @pl.when(end)
+    def _():
+        for n, mm in enumerate(EXTRA):
+            extra_loads[n].wait()
+            cut_blocks(mm, extra_stage.at[n], extra_blocks.at[n])
+            for rel in (1, 2):
+                send(
+                    extra_blocks.at[n, fs_of[rel]], piece_of(mm, f, z_three),
+                    SX, z_slot(mm, rel, z_three), (r, fs_of[rel], t),
+                )
 
     phase("pump_a1")
-    for n, rel in ((1, 3), (2, 1), (2, 2), (2, 3), (3, 1), (3, 2), (3, 3)):
+    for n, rel in ((1, 3), (2, 1), (2, 2), (2, 3)):
         pump(n, rel)
-    arrive(extra_blocks.at[pl.ds(0, 2)], XN)
-    for rel in (1, 2):
-        block = weight_rows(second, fs_of[rel], kept, extra, t)
-        send(block, block, SD, dn(second), partner)
+    phase("z_gates")
+    pump_z((1, 2), middle, gates)
 
     phase("relay_c")
     for h in range(heads):
@@ -469,13 +462,13 @@
             arrive(block, CP + core * 4 + h)
             send(block, block, SC, CC, (r, q, t))
     phase("pump_z0")
-    for n in (0, 1):
-        for rel in (1, 2, 3):
-            pump_z(n, rel)
+    phase("z_ups")
+    pump_z((1, 2), middle, ups)
+    phase("pump_z0")
+    pump_z((0,), end, gates + ups + [(2, soon)])
 
     phase("wait_small")
     local(own_half, own_half, LKEPT).wait()
-    local(own_half.at[0], own_half.at[0], LKEPT).wait()
     target = gathered.at[f, :, lanes(t * local_width, local_width)]
     local(target, target, LKEPT + 1).wait()
     local(wo_half, wo_half, LKEPT + 2).wait()
@@ -515,32 +508,55 @@
                 share(done, SE, EP + (done ^ 1), p)
             for done in (1, 2):
                 share(done, SE + 1, EQ + (done ^ 2), q)
+            phase("z_soon")
+            pump_z((1, 2), middle, [(2, soon)])
+            pump_z((1, 2), end, gates)
         elif k == 3:
             share(3, SE, EP + 2, p)
             relay(1)
             for done in (3, 0):
                 share(done, SE + 1, EQ + (done ^ 2), q)
 
-    phase("pump_z1")
-    pump_z(2, 1)
     phase("relay_e")
     relay(3)
+    phase("z_downs")
+    pump_z((1, 2), middle, [(2, next_), (2, late)])
+    pump_late()
+    pump_z((0,), middle, gates + ups)
+    phase("relay_e")
     relay(0)
-    phase("pump_z15")
-    pump_z(2, 2)
-    phase("relay_e")
     relay(2)
     phase("pump_z2")
-    for n, rel in ((2, 3), (3, 1), (3, 2), (3, 3)):
-        pump_z(n, rel)
+    pump_z((1, 2), end, ups)
+    pump_z((0,), middle, [(2, soon), (2, next_), (2, late)])
+    pump_z((0,), end, [(2, next_)])
+    pump_z((1, 2), end, [(2, soon), (2, next_)])
     phase("wait_w")
     arrive(weights.at[pl.ds(0, 2), :, lanes((1 - t) * units, units)], DN)
 
     gate_scale = jnp.concatenate([gs_all[0, :, own_lanes], gs_all[1, :, own_lanes]], axis=1)
     up_scale = jnp.concatenate([us_all[0, :, own_lanes], us_all[1, :, own_lanes]], axis=1)
 
-    def piece(n):
-        return slice(n * local_width, (n + 1) * local_width)
+    def half_rows(n):
+        return pl.ds(pl.multiple_of(n * local_width, local_width), local_width)
+
+    partner_lanes = lanes((1 - t) * units, units)
+    hiddens = {}
+
+    def down_terms(k, n):
+        term = by_rows(hiddens[k], weights[2, half_rows(n), :])
+        if k == 3:
+            to_p[n] = term.astype(half)
+            send(to_p.at[n], from_p.at[n], SF, FP + n, (r, p, t))
+        elif k == 1:
+            to_p2[n] = term.astype(half)
+            send(to_p2.at[n], from_p2.at[t], SF + 1, FP + 2 + t, (r, p, n))
+        elif k == 0:
+            own_down[n] = term
+        else:
+            arrive(from_p.at[n], FP + n)
+            to_q[n] = (term + from_p[n].astype(jnp.float32)).astype(half)
+            send(to_q.at[n], from_q.at[t], SF + 2, FP + 4 + t, (r, q, n))
 
     for k in (3, 1, 0, 2):
         seq = order[k]
@@ -553,28 +569,23 @@
         normin = (wide * factor * mlp_gain_ref[...]).astype(half)
         gate_pre = jnp.dot(normin, weights[0], preferred_element_type=jnp.float32) * gate_scale
         up_pre = jnp.dot(normin, weights[1], preferred_element_type=jnp.float32) * up_scale
-        hidden = (jax.nn.silu(gate_pre) * up_pre).astype(half)
+        hiddens[k] = (jax.nn.silu(gate_pre) * up_pre).astype(half)
+        if k == 3:
+            phase("wait_half")
+            arrive(weights.at[2, half_rows(0), partner_lanes], DN + 1)
         phase("down")
-        if k == 3:
-            arrive(weights.at[2, :, lanes((1 - t) * units, units)], DN + 1)
-        for n in range(2):
-            term = by_rows(hidden, weights[2, piece(n), :])
-            if k == 3:
-                to_p[n] = term.astype(half)
-                send(to_p.at[n], from_p.at[n], SF, FP + n, (r, p, t))
-            elif k == 1:
-                to_p2[n] = term.astype(half)
-                send(to_p2.at[n], from_p2.at[t], SF + 1, FP + 2 + t, (r, p, n))
-            elif k == 0:
-                own_down[n] = term
-            else:
-                arrive(from_p.at[n], FP + n)
-                to_q[n] = (term + from_p[n].astype(jnp.float32)).astype(half)
-                send(to_q.at[n], from_q.at[t], SF + 2, FP + 4 + t, (r, q, n))
-        if k == 0:
-            send(own_down.at[1 - t], other_down, SO, OUT, partner)
-            far_half = updated.at[f, :, lanes((1 - t) * local_width, local_width)]
-            send(far_half, other_updated, SO + 1, OUT + 1, partner)
+        down_terms(k, 0)
+    phase("z_last")
+    pump_z((0, 1, 2), end, [(2, late)])
+    arrive(weights.at[2, half_rows(1), partner_lanes], DN + 2)
+    phase("down_far")
+    for k in (3, 1, 0):
+        down_terms(k, 1)
+    send(own_down.at[1 - t], other_down, SO, OUT, partner)
+    other_half = updated.at[f, :, lanes((1 - t) * local_width, local_width)]
+    send(other_half, other_updated, SO + 1, OUT + 1, partner)
+    phase("down_q")
+    down_terms(2, 1)
 
     phase("wait_other")
     arrive(other_down, OUT)
@@ -598,24 +609,23 @@
 
     phase("drain")
     for rel in (1, 2, 3):
-        waiter(blocks.at[0], SA + rel - 1, 0).wait_send()
+        waiter(blocks.at[:, 0], SA + rel - 1, 0).wait_send()
     waiter(weights.at[:, :, lanes(t * units, units)], SD, 0).wait_send()
     for n, both in enumerate((os_all, gs_all, us_all)):
         waiter(both.at[t], SS + n, 0).wait_send()
     for n in range(3):
         waiter(own_res.at[0], SR + n, 0).wait_send()
     pl.when(mine == 0)(waiter(own_res.at[0], SR + 3, 0).wait_send)
-    waiter(extra_blocks.at[pl.ds(0, 2)], SX, 0).wait_send()
     for n in range(2):
         waiter(normed, SH + n, 0).wait_send()
     waiter(normed.at[:, pl.ds(0, rows)], SH + 2, 0).wait_send()
-    for index, to, goes, short in z_moves():
-        for length, when in (
-            (3 * own_width, goes & jnp.logical_not(short)),
-            (3 * own_width - 2 * extra, goes & short),
-        ):
-            sent = weights.at[0, pl.ds(0, length), lanes(0, units)]
-            pl.when(when)(waiter(sent, SZ + index, 0).wait_send)
+    for n in range(2):
+        waiter(weights.at[0, pl.ds(0, 9 * quarter), lanes(0, units)], SZ + n, 0).wait_send()
+    left = 18 - 2 * len(EXTRA)
+    relayed = weights.at[0, pl.ds(0, left * quarter), lanes(0, units)]
+    extras = extra_blocks.at[:, pl.ds(0, 2)]
+    pl.when(end)(waiter(extras, SX, 0).wait_send)
+    pl.when(middle)(waiter(relayed, SZ + 2, 0).wait_send)
     waiter(wo_half, SWO, 0).wait_send()
     waiter(gathered.at[0], SC, 0).wait_send()
     for n in range(3):
@@ -678,12 +688,12 @@
             pltpu.VMEM((own_width, local_width), full),
             pltpu.VMEM((local_width, own_width), half),
             pltpu.VMEM((width, own_width), half),
-            pltpu.VMEM((own_width, total_units), full),
-            pltpu.VMEM((2, own_width, units), full),
-            pltpu.VMEM((2, own_width, units), half),
-            pltpu.VMEM((4, own_width, units), half),
-            pltpu.VMEM((own_width // EXTRA_PART, total_units), full),
-            pltpu.VMEM((4, own_width // EXTRA_PART, units), half),
+            pltpu.VMEM((3, own_width // 4, total_units), full),
+            pltpu.VMEM((3, own_width, units), full),
+            pltpu.VMEM((3, own_width, units), half),
+            pltpu.VMEM((3, 4, own_width // 4, units), half),
+            pltpu.VMEM((len(EXTRA), own_width // 4, total_units), full),
+            pltpu.VMEM((len(EXTRA), 4, own_width // 4, units), half),
             pltpu.VMEM((3, width, 2 * units), half),
             pltpu.VMEM((heads, tokens, local_width // heads), half),
             pltpu.VMEM((4, rows, width), half),
@@ -698,9 +708,9 @@
         ]
         + [pltpu.VMEM((2, rows, local_width), half)] * 6
         + [
-            pltpu.SemaphoreType.DMA((29,)),
+            pltpu.SemaphoreType.DMA((28 + len(EXTRA),)),
             pltpu.SemaphoreType.DMA((28,)),
-            pltpu.SemaphoreType.DMA((75,)),
+            pltpu.SemaphoreType.DMA((84,)),
         ],
         compiler_params=pltpu.CompilerParams(
             collective_id=1, has_side_effects=True, vmem_limit_bytes=VMEM_MIB * 2**20

time: 84 us -> 82.6 us (0.983)
  Pallas kernels: 82 us -> 80.5 us
    pallas_call x1, Pallas kernels: 82 us -> 80.5 us  [one_kernel_body(): pl.pallas_call(layer_kernel, out_shape=jax.ShapeDtypeStruct((tokens, loca...]
where the time goes in v4:
time: 82.6 us; the launch traced here: 82.4 us
  Pallas kernels  80.5 us (97%)
  local copies, waits for them, and re-layouts  1.87 us (2%)
    pallas_call x1, Pallas kernels, one_kernel_body(): pl.pallas_call(layer_kernel, out_shape=jax.ShapeDtypeStruct((tokens, loca...  80.5 us
    unnamed x1, local copies, waits for them, and re-layouts  1.87 us

profile of v4, /device:TPU:1, one launch (start us, length us, event | category | flops | bytes accessed | tf_op | source)
XLA Modules:
  0.0 82.4 jit_solution(13559076627971586198)
XLA Ops:
  0.0 80.5 %shard_map.154 = bf16[256,1024]{1,0:T(8,128)(2,1)} custom-call(bf16[256,1024]{1,0:T(8,128)(2,1)} %bitcast.15, bf16[256,1024]{1,0:T(8,128)(2,1)} %bitcast.16, bf16[256,1024]{1,0:T(8,128)(2,1)} %bitcast.17, f32[256,1024]{1,0:T(8,128)} %bitcast.14, bf16[256,1024]{1,0:T(8,128)(2,1)} %bitcast.18, f32[512,1024]{1,0:T(8,128)} %wo_hbm.1, f32[512,1408]{1,0:T(8,128)} %gate_hbm.1, ...), custom_call_target="tpu_custom_call" | custom-call | tf_op jit(solution)/shard_map/pallas_call | solution.py:670
  80.5 1.9 %copy.18 = bf16[1,256,1024]{2,1,0:T(8,128)(2,1)} copy(bf16[1,256,1024]{2,1,0:T(8,128)(2,1)} %bitcast.13) | data formatting | bytes 1048576

commit v5 on v4

--- a/solution.py
+++ b/solution.py
@@ -222,8 +222,8 @@
     head_width = local_width // heads
     starts = [min(j * units, total_units - units) for j in range(4)]
     SA, SD, SS, SR, SH, SZ, SWO, SC, SE, SF, SO, SX = 0, 3, 4, 7, 11, 14, 17, 18, 19, 22, 25, 27
-    A, RES, CP, CQ, CC, CO, WO, SCALE = 0, 9, 10, 18, 19, 20, 21, 22
-    EP, EQ, EC, ZN, DN, FP, OUT = 25, 29, 33, 37, 73, 76, 82
+    A, RES, CP, CQ, CC, CO, WO, SCALE = 0, 9, 10, 14, 15, 16, 17, 18
+    EP, EQ, ZN, DN, FP, OUT = 21, 25, 29, 65, 68, 74
     LSTAGE, LRES, LHEAD, LWO, LOWN, LKEPT, LEND, LSMALL, LEXTRA = 0, 3, 4, 12, 13, 16, 19, 21, 28
 
     def lanes(start, size):
@@ -412,7 +412,7 @@
             for n, to in enumerate((x, y)):
                 send(
                     normed.at[h, pl.ds(core * rows, rows)], target, SH + n,
-                    CP + t * 4 + h if n == core else CQ, (r, to, core),
+                    CP + h if n == core else CQ, (r, to, core),
                 )
         send(normed.at[h, other_rows], target, SH + 2, CO, partner)
         local(normed.at[h, my_rows], target, LKEPT + 1).start()
@@ -457,9 +457,9 @@
 
     phase("relay_c")
     for h in range(heads):
+        arrive(gathered.at[p, :, lanes(0, 2 * head_width)], CP + h)
         for core in range(2):
             block = gathered.at[p, :, head_lanes(core, h)]
-            arrive(block, CP + core * 4 + h)
             send(block, block, SC, CC, (r, q, t))
     phase("pump_z0")
     phase("z_ups")
@@ -489,7 +489,7 @@
     def relay(k):
         block = updated.at[order[k], :, feature_lanes(p)]
         arrive(block, EP + k)
-        send(block, block, SE + 2, EC + (k ^ 2), (r, q, t))
+        send(block, block, SE + 2, EQ + (k ^ 2), (r, q, t))
 
     for k in range(4):
         seq = order[k]
@@ -529,8 +529,6 @@
     phase("pump_z2")
     pump_z((1, 2), end, ups)
     pump_z((0,), middle, [(2, soon), (2, next_), (2, late)])
-    pump_z((0,), end, [(2, next_)])
-    pump_z((1, 2), end, [(2, soon), (2, next_)])
     phase("wait_w")
     arrive(weights.at[pl.ds(0, 2), :, lanes((1 - t) * units, units)], DN)
 
@@ -561,8 +559,7 @@
     for k in (3, 1, 0, 2):
         seq = order[k]
         phase("wait_e")
-        arrive(updated.at[seq, :, feature_lanes(q)], EQ + k)
-        arrive(updated.at[seq, :, feature_lanes(c)], EC + k)
+        arrive(updated.at[seq, :, lanes(0, 2 * own_width)], EQ + k)
         phase("gate_up")
         wide = updated[seq].astype(jnp.float32)
         factor = lax.rsqrt(jnp.mean(wide * wide, axis=-1, keepdims=True) + epsilon)
@@ -571,6 +568,9 @@
         up_pre = jnp.dot(normin, weights[1], preferred_element_type=jnp.float32) * up_scale
         hiddens[k] = (jax.nn.silu(gate_pre) * up_pre).astype(half)
         if k == 3:
+            phase("z_half")
+            pump_z((0,), end, [(2, next_)])
+            pump_z((1, 2), end, [(2, soon), (2, next_)])
             phase("wait_half")
             arrive(weights.at[2, half_rows(0), partner_lanes], DN + 1)
         phase("down")
@@ -710,7 +710,7 @@
         + [
             pltpu.SemaphoreType.DMA((28 + len(EXTRA),)),
             pltpu.SemaphoreType.DMA((28,)),
-            pltpu.SemaphoreType.DMA((84,)),
+            pltpu.SemaphoreType.DMA((76,)),
         ],
         compiler_params=pltpu.CompilerParams(
             collective_id=1, has_side_effects=True, vmem_limit_bytes=VMEM_MIB * 2**20

time: 82.6 us -> 81.5 us (0.987)
  Pallas kernels: 80.5 us -> 79.5 us
    pallas_call x1, Pallas kernels: 80.5 us -> 79.5 us  [one_kernel_body(): pl.pallas_call(layer_kernel, out_shape=jax.ShapeDtypeStruct((tokens, loca...]
where the time goes in v5:
time: 81.5 us; the launch traced here: 81.4 us
  Pallas kernels  79.5 us (98%)
  local copies, waits for them, and re-layouts  1.87 us (2%)
    pallas_call x1, Pallas kernels, one_kernel_body(): pl.pallas_call(layer_kernel, out_shape=jax.ShapeDtypeStruct((tokens, loca...  79.5 us
    unnamed x1, local copies, waits for them, and re-layouts  1.87 us

profile of v5, /device:TPU:1, one launch (start us, length us, event | category | flops | bytes accessed | tf_op | source)
XLA Modules:
  0.0 81.4 jit_solution(4541157592650575526)
XLA Ops:
  0.0 79.5 %shard_map.154 = bf16[256,1024]{1,0:T(8,128)(2,1)} custom-call(bf16[256,1024]{1,0:T(8,128)(2,1)} %bitcast.15, bf16[256,1024]{1,0:T(8,128)(2,1)} %bitcast.16, bf16[256,1024]{1,0:T(8,128)(2,1)} %bitcast.17, f32[256,1024]{1,0:T(8,128)} %bitcast.14, bf16[256,1024]{1,0:T(8,128)(2,1)} %bitcast.18, f32[512,1024]{1,0:T(8,128)} %wo_hbm.1, f32[512,1408]{1,0:T(8,128)} %gate_hbm.1, ...), custom_call_target="tpu_custom_call" | custom-call | tf_op jit(solution)/shard_map/pallas_call | solution.py:670
  79.5 1.9 %copy.18 = bf16[1,256,1024]{2,1,0:T(8,128)(2,1)} copy(bf16[1,256,1024]{2,1,0:T(8,128)(2,1)} %bitcast.13) | data formatting | bytes 1048576

commit v6 on v5

--- a/solution.py
+++ b/solution.py
@@ -575,8 +575,10 @@
             arrive(weights.at[2, half_rows(0), partner_lanes], DN + 1)
         phase("down")
         down_terms(k, 0)
+        if k == 0:
+            pump_z((1, 2), end, [(2, late)])
     phase("z_last")
-    pump_z((0, 1, 2), end, [(2, late)])
+    pump_z((0,), end, [(2, late)])
     arrive(weights.at[2, half_rows(1), partner_lanes], DN + 2)
     phase("down_far")
     for k in (3, 1, 0):

time: 81.5 us -> 81.5 us (level)
  no operation moved by 1% of the time
where the time goes in v6:
time: 81.5 us; the launch traced here: 81.4 us
  Pallas kernels  79.5 us (98%)
  local copies, waits for them, and re-layouts  1.87 us (2%)
    pallas_call x1, Pallas kernels, one_kernel_body(): pl.pallas_call(layer_kernel, out_shape=jax.ShapeDtypeStruct((tokens, loca...  79.5 us
    unnamed x1, local copies, waits for them, and re-layouts  1.87 us

profile of v6, /device:TPU:1, one launch (start us, length us, event | category | flops | bytes accessed | tf_op | source)
XLA Modules:
  0.0 81.4 jit_solution(14474782190913395635)
XLA Ops:
  0.0 79.5 %shard_map.154 = bf16[256,1024]{1,0:T(8,128)(2,1)} custom-call(bf16[256,1024]{1,0:T(8,128)(2,1)} %bitcast.15, bf16[256,1024]{1,0:T(8,128)(2,1)} %bitcast.16, bf16[256,1024]{1,0:T(8,128)(2,1)} %bitcast.17, f32[256,1024]{1,0:T(8,128)} %bitcast.14, bf16[256,1024]{1,0:T(8,128)(2,1)} %bitcast.18, f32[512,1024]{1,0:T(8,128)} %wo_hbm.1, f32[512,1408]{1,0:T(8,128)} %gate_hbm.1, ...), custom_call_target="tpu_custom_call" | custom-call | tf_op jit(solution)/shard_map/pallas_call | solution.py:672
  79.5 1.9 %copy.18 = bf16[1,256,1024]{2,1,0:T(8,128)(2,1)} copy(bf16[1,256,1024]{2,1,0:T(8,128)(2,1)} %bitcast.13) | data formatting | bytes 1048576
